TPU v7x, 32 devices: a whole 2x2x4 slice. The times are simulated.
32 devices in a mesh: sp: 8 (over z, y), tp: 4 (over x, core).
Axes of the slice: x: 2, y: 2, z: 4, core: 2. Of those that a mesh axis runs over, the one named last changes fastest.
Arguments:
- tokens: bfloat16 [4096, 2048], P(('sp', 'tp')), may hold values from -6 to 6
- norm_gain: float32 [2048], replicated, may hold values from 0.1 to 1.9
- query_weight: bfloat16 [2048, 2048], P('sp', 'tp'), may hold values from -0.125 to 0.125
- key_weight: bfloat16 [2048, 2048], P('sp', 'tp'), may hold values from -0.125 to 0.125
- value_weight: bfloat16 [2048, 4096], P('sp', 'tp'), may hold values from -0.125 to 0.125
- retain_gate: bfloat16 [2048, 4096], P('sp', 'tp'), may hold values from -0.125 to 0.125
- unit_value: bfloat16 [2048, 2048], P('sp', 'tp'), may hold values from -0.125 to 0.125
- unit_gate: bfloat16 [2048, 2048], P('sp', 'tp'), may hold values from -0.125 to 0.125
- convolve_gate: bfloat16 [2048, 2048], P('sp', 'tp'), may hold values from -0.125 to 0.125
- filter_taps: float32 [31, 2048], replicated, may hold values from -1 to 1
- layer_gain: float32 [2048], replicated, may hold values from 0.1 to 1.9
- layer_shift: float32 [2048], replicated, may hold values from -3 to 3
- retain_output: bfloat16 [2048, 4096], P('sp', 'tp'), may hold values from -0.09375 to 0.09375
- convolve_output: bfloat16 [2048, 2048], P('sp', 'tp'), may hold values from -0.125 to 0.125
Outputs:
- mixed: bfloat16 [4096, 2048], P(('sp', 'tp'))
All inputs are finite; a program needn't handle non-finite values.
Results may differ from a plain program's by a relative error of at most 0.018.
Values may be sent and summed in bfloat16 or wider, within the bound.
A program may use at most 128 MiB of HBM per device.

v0:
```python
import jax
import jax.numpy as jnp
from jax import lax
from jax.experimental import pallas as pl
from jax.experimental.pallas import tpu as pltpu
from jax.sharding import Mesh
from jax.sharding import PartitionSpec as P

KEY = 256
VAL = 512
GROUP = 512
KW = 31


rms_eps = 1e-06
group_eps = 1.0
layer_eps = 0.001
rope_base = 10000.0


SPANS = ("tp", "lo")


def swap_planes(x):
    size = lax.axis_size("tp")
    pairs = [(h * size + t, t * size + h) for h in range(size) for t in range(size)]
    return lax.ppermute(x, ("hi", "tp"), pairs)


def from_behind(x, by):
    outer, inner = lax.axis_size("tp"), lax.axis_size("lo")
    spot = [(i % inner) * outer + i // inner for i in range(outer * inner)]
    return lax.ppermute(x, ("lo", "tp"), list(zip(spot[:-by], spot[by:])))


def carried_in(contribution, log_span_decay):
    length = lax.axis_size(SPANS)
    state = from_behind(contribution.astype(jnp.bfloat16), 1).astype(jnp.float32)
    by = 1
    while by < length:
        earlier = from_behind(state.astype(jnp.bfloat16), by).astype(jnp.float32)
        state = state + jnp.exp(log_span_decay * by)[:, None, None] * earlier
        by *= 2
    return state


def spread_kernel(count, *refs):
    rows_ref, blocks = refs[0], refs[1 : 1 + count]
    tokens_out, fulls = refs[1 + count], refs[2 + count : 2 + 2 * count]
    passing = refs[2 + 2 * count : 2 + 3 * count]
    bounce = refs[2 + 3 * count : 2 + 4 * count]
    rows_bounce, send, arrive, arrive_pass, send_rows, arrive_rows, own = refs[2 + 4 * count :]
    hi, lo, tp = lax.axis_index("hi"), lax.axis_index("lo"), lax.axis_index("tp")
    planes = lax.axis_size("hi")
    side, core = tp // 2, tp % 2
    far_side = 1 - side
    across = (hi, lo, 2 * far_side + core)
    beside = (hi, 1 - lo, tp)
    sibling = (hi, lo, 2 * side + 1 - core)
    held = lax.rem(side + hi // 2, 2)
    other_held = 1 - held

    def remote(source, target, out_sem, in_sem, device):
        return pltpu.make_async_remote_copy(
            src_ref=source,
            dst_ref=target,
            send_sem=out_sem,
            recv_sem=in_sem,
            device_id=device,
            device_id_type=pl.DeviceIdType.MESH,
        )

    def via_vmem(source, buffer, target, done):
        inward = pltpu.make_async_copy(source, buffer, own)
        inward.start()
        inward.wait()
        pltpu.make_async_copy(buffer, target, done).start()

    def piece(k, source, row, half):
        depth = blocks[k].shape[0]
        start = (source * 2 + row) * depth + half * (depth // 2)
        return fulls[k].at[pl.ds(pl.multiple_of(start, depth // 2), depth // 2)]

    def half_of(k, half):
        depth = blocks[k].shape[0] // 2
        return blocks[k].at[pl.ds(half * depth, depth)]

    waits = []

    def push(k, source, row, half, slot, device):
        part = piece(k, source, row, half)
        copy = remote(part, part, send.at[k, slot], arrive.at[k, source, row, half], device)
        copy.start()
        waits.append(copy)

    def landed(k, source, row, half):
        part = piece(k, source, row, half)
        remote(part, part, send.at[k, 0], arrive.at[k, source, row, half], across).wait_recv()

    landing = pl.multiple_of(tp * rows_ref.shape[0], rows_ref.shape[0])
    my_rows = tokens_out.at[pl.ds(landing, rows_ref.shape[0])]

    for k in range(count):
        copy = remote(half_of(k, 1), passing[k], send.at[k, 0], arrive_pass.at[k], across)
        copy.start()
        waits.append(copy)

    def first_entry(k):
        return remote(
            half_of(k, 0),
            piece(k, hi, lo, 0),
            send.at[k, 1],
            arrive.at[k, hi, lo, 0],
            (tp, lo, 2 * side + lax.rem(hi, 2)),
        )

    def second_entry(k):
        return remote(
            passing[k],
            piece(k, hi, lo, 1),
            send.at[k, 2],
            arrive.at[k, hi, lo, 1],
            (2 * far_side + core, lo, 2 * side + lax.rem(hi, 2)),
        )

    def rows_copy(step):
        target = lax.rem(hi + step, planes)
        return remote(
            rows_ref, my_rows, send_rows.at[step], arrive_rows.at[tp], (target, lo, hi)
        )

    stays_first = tp == hi
    stays_second = 2 * far_side + core == hi
    for k in range(count):

        @pl.when(jnp.logical_not(stays_first))
        def _():
            first_entry(k).start()

    for step in range(1, 4):
        rows_copy(step).start()

    @pl.when(jnp.logical_not(stays_first))
    def _():
        rows_copy(0).start()

    @pl.when(stays_first)
    def _():
        via_vmem(rows_ref, rows_bounce, my_rows, arrive_rows.at[tp])
        for k in range(count):
            via_vmem(half_of(k, 0), bounce[k], piece(k, hi, lo, 0), arrive.at[k, hi, lo, 0])

    for k in range(count):
        remote(passing[k], passing[k], send.at[k, 0], arrive_pass.at[k], across).wait_recv()

        @pl.when(jnp.logical_not(stays_second))
        def _():
            second_entry(k).start()

        @pl.when(stays_second)
        def _():
            via_vmem(passing[k], bounce[k], piece(k, hi, lo, 1), arrive.at[k, hi, lo, 1])

    def own_step(k):
        for n in range(2):
            source = core + 2 * n
            landed(k, source, lo, held)
            push(k, source, lo, held, 3 + 3 * n, across)
            push(k, source, lo, held, 4 + 3 * n, beside)
            push(k, source, lo, held, 5 + 3 * n, sibling)

    def near_step(k):
        landed(k, core, lo, other_held)
        push(k, core, lo, other_held, 9, beside)
        push(k, core, lo, other_held, 10, sibling)
        landed(k, core + 2, 1 - lo, held)
        push(k, core + 2, 1 - lo, held, 11, across)
        push(k, core + 2, 1 - lo, held, 12, sibling)
        landed(k, core + 2, lo, other_held)
        push(k, core + 2, lo, other_held, 13, sibling)
        landed(k, core, 1 - lo, held)
        push(k, core, 1 - lo, held, 14, sibling)

    def far_step(k):
        landed(k, core, 1 - lo, other_held)
        push(k, core, 1 - lo, other_held, 15, sibling)
        landed(k, core + 2, 1 - lo, other_held)
        push(k, core + 2, 1 - lo, other_held, 16, sibling)

    for step in range(count + 2):
        if step < count:
            own_step(step)
        if 0 <= step - 1 < count:
            near_step(step - 1)
        if 0 <= step - 2:
            far_step(step - 2)

    for k in range(count):
        for n in range(2):
            for row in range(2):
                for half in range(2):
                    landed(k, 1 - core + 2 * n, row, half)
    for t in range(4):
        part = tokens_out.at[pl.ds(t * rows_ref.shape[0], rows_ref.shape[0])]
        remote(part, part, send_rows.at[0], arrive_rows.at[t], across).wait_recv()
    for copy in waits:
        copy.wait_send()
    for step in range(1, 4):
        rows_copy(step).wait_send()

    @pl.when(jnp.logical_not(stays_first))
    def _():
        rows_copy(0).wait_send()
        for k in range(count):
            first_entry(k).wait_send()

    @pl.when(jnp.logical_not(stays_second))
    def _():
        for k in range(count):
            second_entry(k).wait_send()


def spread(rows, blocks):
    count = len(blocks)
    shares = lax.axis_size(SPANS)
    halves = [(b.shape[0] // 2, b.shape[1]) for b in blocks]
    outs = [jax.ShapeDtypeStruct((4 * rows.shape[0], rows.shape[1]), rows.dtype)]
    outs += [jax.ShapeDtypeStruct((shares * b.shape[0], b.shape[1]), b.dtype) for b in blocks]
    outs += [jax.ShapeDtypeStruct(h, b.dtype) for h, b in zip(halves, blocks)]
    results = pl.pallas_call(
        lambda *refs: spread_kernel(count, *refs),
        out_shape=outs,
        in_specs=[pl.BlockSpec(memory_space=pl.ANY)] * (1 + count),
        out_specs=[pl.BlockSpec(memory_space=pl.ANY)] * len(outs),
        scratch_shapes=[pltpu.VMEM(h, b.dtype) for h, b in zip(halves, blocks)]
        + [
            pltpu.VMEM(rows.shape, rows.dtype),
            pltpu.SemaphoreType.DMA((count, 17)),
            pltpu.SemaphoreType.DMA((count, 4, 2, 2)),
            pltpu.SemaphoreType.DMA((count,)),
            pltpu.SemaphoreType.DMA((4,)),
            pltpu.SemaphoreType.DMA((4,)),
            pltpu.SemaphoreType.DMA,
        ],
        compiler_params=pltpu.CompilerParams(has_side_effects=True),
        name="spread",
    )(rows, *blocks)
    return results[0], results[1 : 1 + count]


def rms_normalize(tokens, norm_gain):
    widened = tokens.astype(jnp.float32)
    scaled = widened * lax.rsqrt(jnp.mean(widened * widened, axis=-1, keepdims=True) + rms_eps)
    return (scaled * norm_gain).astype(jnp.bfloat16)


def rotate(vectors, positions):
    half_width = vectors.shape[-1] // 2
    frequency = rope_base ** (-jnp.arange(half_width, dtype=jnp.float32) / half_width)
    angles = positions.astype(jnp.float32)[:, None] * frequency
    cosine = jnp.cos(angles)[:, None, :]
    sine_part = jnp.sin(angles)[:, None, :]
    front_half = vectors[..., :half_width]
    back_half = vectors[..., half_width:]
    return jnp.concatenate(
        [front_half * cosine - back_half * sine_part, front_half * sine_part + back_half * cosine],
        axis=-1,
    )


def prepare(queries, key_rows, values, positions):
    row_count = queries.shape[0]
    rotated_query = rotate(
        queries.astype(jnp.float32).reshape(row_count, -1, KEY), positions
    ).astype(jnp.bfloat16)
    rotated_keys = (
        rotate(key_rows.astype(jnp.float32).reshape(row_count, -1, KEY), positions) * KEY ** (-0.5)
    ).astype(jnp.bfloat16)
    value_heads = values.reshape(row_count, -1, VAL)
    return (rotated_query, rotated_keys, value_heads)


def decay_logs(first_head, head_total, all_heads, seq_length):
    ratio = (first_head + jnp.arange(head_total)).astype(jnp.float32) / (all_heads - 1)
    return (jnp.log(0.05) + ratio * jnp.log(18.0)) / seq_length


def local_parts(queries, key_rows, values, log_decay):
    row_count = queries.shape[0]
    indices = jnp.arange(row_count, dtype=jnp.float32)
    offsets = indices[:, None] - indices[None, :]
    causal = offsets >= 0
    weight = jnp.where(
        causal[None], jnp.exp(log_decay[:, None, None] * jnp.where(causal, offsets, 0.0)[None]), 0.0
    )
    scores = (
        jnp.einsum("ihd,jhd->hij", queries, key_rows, preferred_element_type=jnp.float32) * weight
    ).astype(jnp.bfloat16)
    within = jnp.einsum("hij,jhe->ihe", scores, values, preferred_element_type=jnp.float32)
    trailing = jnp.exp(log_decay[None, :] * (row_count - 1.0 - indices)[:, None])
    weighted = (key_rows.astype(jnp.float32) * trailing[:, :, None]).astype(jnp.bfloat16)
    contribution = jnp.einsum("jhd,jhe->hde", weighted, values, preferred_element_type=jnp.float32)
    return (within, contribution)


def cross_part(queries, carry_state, log_decay):
    row_count = queries.shape[0]
    indices = jnp.arange(row_count, dtype=jnp.float32)
    leading = jnp.exp(log_decay[None, :] * (indices + 1.0)[:, None])
    return (
        jnp.einsum(
            "ihd,hde->ihe",
            queries,
            carry_state.astype(jnp.bfloat16),
            preferred_element_type=jnp.float32,
        )
        * leading[:, :, None]
    )


def retain_finish(raw, switch):
    average = jnp.mean(raw, axis=-1, keepdims=True)
    spread = jnp.mean(jnp.square(raw - average), axis=-1, keepdims=True)
    normalized = ((raw - average) * lax.rsqrt(spread + group_eps)).reshape(raw.shape[0], -1)
    return (normalized * jax.nn.silu(switch.astype(jnp.float32))).astype(jnp.bfloat16)


def convolve_branch(gated_input, before, tap_slice, gain_slice, shift_slice, switch):
    padded = jnp.concatenate([before, gated_input], axis=0)
    row_count = gated_input.shape[0]
    summed = jnp.zeros(gated_input.shape, jnp.float32)
    for tap_index in range(tap_slice.shape[0]):
        summed = (
            summed
            + padded[tap_index : tap_index + row_count].astype(jnp.float32) * tap_slice[tap_index]
        )
    grouped = summed.reshape(row_count, -1, GROUP)
    average = jnp.mean(grouped, axis=-1, keepdims=True)
    spread = jnp.mean(jnp.square(grouped - average), axis=-1, keepdims=True)
    normalized = ((grouped - average) * lax.rsqrt(spread + layer_eps)).reshape(row_count, -1)
    normalized = normalized * gain_slice + shift_slice
    return (jax.nn.silu(normalized) * jax.nn.silu(switch.astype(jnp.float32))).astype(jnp.bfloat16)


def contract(hidden, matrix):
    return lax.dot_general(
        hidden, matrix, (((1,), (1,)), ((), ())), preferred_element_type=jnp.float32
    )


def local(
    tokens,
    norm_gain,
    query_weight,
    key_weight,
    value_weight,
    retain_gate,
    unit_value,
    unit_gate,
    convolve_gate,
    filter_taps,
    layer_gain,
    layer_shift,
    retain_output,
    convolve_output,
):
    head_groups = lax.axis_size("hi")
    chain_length = lax.axis_size(SPANS)
    head_rank = lax.axis_index("hi")
    chain_rank = lax.axis_index(SPANS)
    def project(rows, merged, *matrices):
        product = jnp.dot(rows, merged, preferred_element_type=jnp.float32).astype(jnp.bfloat16)
        ends = [sum(m.shape[1] for m in matrices[: k + 1]) for k in range(len(matrices) - 1)]
        return jnp.split(product, ends, axis=1)

    first = (key_weight, value_weight, query_weight)
    second = (unit_value, unit_gate, convolve_gate, retain_gate)
    third = (retain_output, convolve_output)
    groups = (first, second, third)
    merged = [jnp.concatenate(group, axis=1) for group in groups]
    normed = rms_normalize(tokens, norm_gain)
    if (lax.axis_size("lo"), lax.axis_size("tp")) == (2, 4):
        normed, merged = spread(normed, merged)
    else:
        normed = lax.all_gather(swap_planes(normed), "hi", axis=0, tiled=True)
        merged = [lax.all_gather(swap_planes(m), SPANS, axis=0, tiled=True) for m in merged]
    key_rows, values, queries = project(normed, merged[0], *first)
    glu_value, glu_switch, convolve_switch, retain_switch = project(normed, merged[1], *second)
    out_full = merged[2]
    row_count = normed.shape[0]
    local_heads = queries.shape[1] // KEY
    positions = chain_rank * row_count + jnp.arange(row_count, dtype=jnp.int32)
    rotated_query, rotated_keys, value_heads = prepare(queries, key_rows, values, positions)
    log_decay = decay_logs(
        head_rank * local_heads, local_heads, local_heads * head_groups, row_count * chain_length
    )
    within, contribution = local_parts(rotated_query, rotated_keys, value_heads, log_decay)
    gated_input = (
        glu_value.astype(jnp.float32) * jax.nn.sigmoid(glu_switch.astype(jnp.float32))
    ).astype(jnp.bfloat16)
    channels = gated_input.shape[1]
    before = from_behind(gated_input[row_count - (KW - 1) :], 1)
    incoming = carried_in(contribution, log_decay * row_count)
    raw = within + cross_part(rotated_query, incoming, log_decay)
    retain_hidden = retain_finish(raw, retain_switch)
    tap_slice = lax.dynamic_slice_in_dim(filter_taps, head_rank * channels, channels, 1)
    gain_slice = lax.dynamic_slice_in_dim(layer_gain, head_rank * channels, channels, 0)
    shift_slice = lax.dynamic_slice_in_dim(layer_shift, head_rank * channels, channels, 0)
    convolve_hidden = convolve_branch(
        gated_input, before, tap_slice, gain_slice, shift_slice, convolve_switch
    )
    hidden = jnp.concatenate([retain_hidden, convolve_hidden], axis=1)
    mixed = contract(hidden, out_full).astype(jnp.bfloat16)
    return swap_planes(lax.psum_scatter(mixed, "hi", scatter_dimension=0, tiled=True))


def solution(mesh):
    sp, tp = mesh.shape["sp"], mesh.shape["tp"]
    planes = Mesh(mesh.devices.reshape(tp, sp // tp, tp), ("hi", "lo", "tp"))
    return jax.shard_map(
        local,
        mesh=planes,
        in_specs=(
            P(("hi", "lo", "tp"), None),
            P(),
            P(("hi", "lo"), "tp"),
            P(("hi", "lo"), "tp"),
            P(("hi", "lo"), "tp"),
            P(("hi", "lo"), "tp"),
            P(("hi", "lo"), "tp"),
            P(("hi", "lo"), "tp"),
            P(("hi", "lo"), "tp"),
            P(),
            P(),
            P(),
            P(("hi", "lo"), "tp"),
            P(("hi", "lo"), "tp"),
        ),
        out_specs=P(("hi", "lo", "tp"), None),
        check_vma=False,
    )
```

profile of v0, /device:TPU:2, one launch (start us, length us, event | category | flops | bytes accessed | tf_op | source)
XLA Modules:
  0.0 371.6 jit_solution(10417067874516821925)
XLA Ops:
  6.6 1.3 fusion.10
  8.0 2.2 pad_maximum_fusion.2.refs_3_
  13.5 179.5 %spread.1 = (bf16[512,2048]{1,0:T(8,128)(2,1)}, bf16[2048,2048]{1,0:T(8,128)(2,1)}, bf16[2048,2560]{1,0:T(8,128)(2,1)}, bf16[2048,1536]{1,0:T(8,128)(2,1)}, bf16...) custom-call(bf16[128,2048]{1,0:T(8,128)(2,1)} %fusion.12.refs_0_, ...), custom_call_target="tpu_custom_call" | custom-call | tf_op jit(solution)/shard_map/spread/pallas_call | solution.py:230
  192.9 8.5 %convolution_convert_fusion.2 = bf16[512,2048]{1,0:T(8,128)(2,1)S(1)} fusion(bf16[512,2048]{1,0:T(8,128)(2,1)} %get-tuple-element.9, bf16[2048,2048]{1,0:T(8,128)(2,1)} %get-tuple-element.10), kind=kOutput, calls=%fused_computation.31 | convolution fusion | flops 4296015872 | bytes 12582912 | tf_op jit(solution)/shard_map/dot_general | solution.py:372
  208.0 2.4 collective-permute-start
  210.4 10.9 %convolution_convert_fusion = bf16[512,2560]{1,0:T(8,128)(2,1)} fusion(bf16[512,2048]{1,0:T(8,128)(2,1)S(1)} %copy-done.20, bf16[2048,2560]{1,0:T(8,128)(2,1)} %get-tuple-element.11), kind=kOutput, calls=%fused_computation.29 | convolution fusion | flops 5370019840 | bytes 15204352 | tf_op jit(solution)/shard_map/dot_general | solution.py:372
  221.4 1.5 multiply_convert_fusion.1
  222.9 3.6 collective-permute-start.4
  228.8 1.8 constant_dynamic-slice_fusion
  231.0 2.2 collective-permute-start.1
  233.7 1.3 dynamic_slice.10
  235.1 1.3 dynamic_slice.11
  237.6 4.2 %fusion.9 = f32[2,512,512]{2,1,0:T(8,128)} fusion(f32[512,512]{1,0:T(8,128)} %fusion.23, f32[2]{0:T(128)} %copy-done.19, pred[512,512]{1,0:T(8,128)(4,1)S(1)} %fusion.24, bf16[64,2,8,512]{3,2,1,0:T(8,128)(2,1)S(1)} %bitcast.51, bf16[512,2,128]{2,0,1:T(8,128)(2,1)S(1)} %get-tuple-element.25, bf16[512,2,128]{2,0,1:T(8,128)(2,1)S(1)} %get-tuple-element.26, ...), kind=kOutput, calls=%fused_computation.47 | convolution fusion | flops 809238528 | bytes 6029320 | tf_op jit(solution)/shard_map/hij,jhe->ihe/dot_general | solution.py:299
  241.8 1.4 collective-permute-done.1
  244.0 4.5 %collective-permute-start.2 = (bf16[2,256,512]{2,1,0:T(8,128)(2,1)S(1)}, bf16[2,256,512]{2,1,0:T(8,128)(2,1)S(1)}, u32[]{:S(2)}, u32[]{:S(2)}) collective-permute-start(bf16[2,256,512]{2,1,0:T(8,128)(2,1)S(1)} %fusion.27), channel_id=1, source_target_pairs={{0,1},{4,5},{1,2},{5,6},{2,3},{6,7},{8,9},{12,13},{9,10},{13,14},{... | collective-permute-start | bytes 1572872 | tf_op jit(solution)/shard_map/ppermute | solution.py:33
  248.5 5.6 %fusion.78 = (f32[512]{0:T(512)S(1)}, f32[512,512]{1,0:T(8,128)S(1)}) fusion(f32[512]{0:T(512)S(1)} %bitcast.64, bf16[512,512]{1,0:T(8,128)(2,1)S(1)} %multiply_convert_fusion.1, f32[512]{0:T(512)S(1)} %bitcast.66, bf16[30,512]{1,0:T(8,128)(2,1)S(1)} %collective-permute-done.4, f32[512]{0:T(512)S(1)} %bitcast.67, f32[512]{0:T(512)S(1)} %bitcast.68, ...), kind=kLoop, calls=%fused_computation.159 | loop fusion | flops 47971840 | bytes 1669120 | tf_op jit(solution)/shard_map/reduce_sum | solution.py:338
  257.2 2.5 fusion.25
  259.7 10.3 %collective-permute-done.3 = bf16[2,256,512]{2,1,0:T(8,128)(2,1)S(1)} collective-permute-done((bf16[2,256,512]{2,1,0:T(8,128)(2,1)S(1)}, bf16[2,256,512]{2,1,0:T(8,128)(2,1)S(1)}, u32[]{:S(2)}, u32[]{:S(2)}) %collective-permute-start.3) | collective-permute-done | bytes 524320 | tf_op jit(solution)/shard_map/ppermute | solution.py:33
  271.6 1.8 copy.23
  273.4 2.6 fusion.5
  276.0 7.4 %convolution_convert_fusion.1 = bf16[512,2048]{1,0:T(8,128)(2,1)} fusion(bf16[2048,1536]{1,0:T(8,128)(2,1)} %get-tuple-element.12, bf16[512,512]{1,0:T(8,128)(2,1)S(1)} %copy-done.5, bf16[512,1024]{1,0:T(8,128)(2,1)S(1)} %fusion.5), kind=kOutput, calls=%fused_computation.30 | convolution fusion | flops 3225419776 | bytes 9961472 | tf_op jit(solution)/shard_map/dot_general | solution.py:346
  283.4 52.8 %reduce-scatter.2.cloned.1.call-done = bf16[128,2048]{1,0:T(8,128)(2,1)} async-done(((bf16[512,2048]{1,0:T(8,128)(2,1)}), bf16[128,2048]{1,0:T(8,128)(2,1)}) %reduce-scatter.2.cloned.1.call-update) | async-done | bytes 524304 | tf_op jit(solution)/shard_map/reduce_scatter | solution.py:414
  336.2 3.5 collective-permute-start.5
  339.8 24.3 %collective-permute-done.5 = bf16[128,2048]{1,0:T(8,128)(2,1)S(1)} collective-permute-done((bf16[128,2048]{1,0:T(8,128)(2,1)}, bf16[128,2048]{1,0:T(8,128)(2,1)S(1)}, u32[]{:S(2)}, u32[]{:S(2)}) %collective-permute-start.5) | collective-permute-done | bytes 524320 | tf_op jit(solution)/shard_map/ppermute | solution.py:27
  (83 shorter events, 20.3 us)
Async XLA Ops:
  6.5 3.6 copy-start.1
  6.5 3.6 copy-start.13
  6.5 4.6 %copy-start.11 = (bf16[256,512]{1,0:T(8,128)(2,1)S(1)}, bf16[256,512]{1,0:T(8,128)(2,1)}, u32[]{:S(2)}) copy-start(bf16[256,512]{1,0:T(8,128)(2,1)} %param.16) | copy-start | bytes 786436
  6.5 4.6 %copy-start.12 = (bf16[256,512]{1,0:T(8,128)(2,1)S(1)}, bf16[256,512]{1,0:T(8,128)(2,1)}, u32[]{:S(2)}) copy-start(bf16[256,512]{1,0:T(8,128)(2,1)} %param.17) | copy-start | bytes 786436
  6.5 4.6 %copy-start.4 = (bf16[256,1024]{1,0:T(8,128)(2,1)S(1)}, bf16[256,1024]{1,0:T(8,128)(2,1)}, u32[]{:S(2)}) copy-start(bf16[256,1024]{1,0:T(8,128)(2,1)} %param.18) | copy-start | bytes 1572868
  6.5 329.7 %reduce-scatter.2.cloned.1.call-start = ((), (), s32[]{:S(2)}) async-start(), calls=%async_computation.1 | async-start | bytes 2621440 | tf_op jit(solution)/shard_map/reduce_scatter | solution.py:414
  8.0 4.3 %copy-start.3 = (bf16[256,1024]{1,0:T(8,128)(2,1)S(1)}, bf16[256,1024]{1,0:T(8,128)(2,1)}, u32[]{:S(2)}) copy-start(bf16[256,1024]{1,0:T(8,128)(2,1)} %param.19) | copy-start | bytes 1572868
  8.0 4.3 %copy-start.8 = (bf16[256,512]{1,0:T(8,128)(2,1)S(1)}, bf16[256,512]{1,0:T(8,128)(2,1)}, u32[]{:S(2)}) copy-start(bf16[256,512]{1,0:T(8,128)(2,1)} %param.22) | copy-start | bytes 786436
  8.0 4.3 %copy-start.9 = (bf16[256,512]{1,0:T(8,128)(2,1)S(1)}, bf16[256,512]{1,0:T(8,128)(2,1)}, u32[]{:S(2)}) copy-start(bf16[256,512]{1,0:T(8,128)(2,1)} %param.21) | copy-start | bytes 786436
  8.0 4.3 %copy-start.10 = (bf16[256,512]{1,0:T(8,128)(2,1)S(1)}, bf16[256,512]{1,0:T(8,128)(2,1)}, u32[]{:S(2)}) copy-start(bf16[256,512]{1,0:T(8,128)(2,1)} %param.20) | copy-start | bytes 786436
  206.4 4.0 %copy-start.20 = (bf16[512,2048]{1,0:T(8,128)(2,1)S(1)}, bf16[512,2048]{1,0:T(8,128)(2,1)}, u32[]{:S(2)}) copy-start(bf16[512,2048]{1,0:T(8,128)(2,1)} %get-tuple-element.9) | copy-start | bytes 6291460
  208.0 23.0 %collective-permute-start = (bf16[2,256,512]{2,1,0:T(8,128)(2,1)S(1)}, bf16[2,256,512]{2,1,0:T(8,128)(2,1)S(1)}, u32[]{:S(2)}, u32[]{:S(2)}) collective-permute-start(bf16[2,256,512]{2,1,0:T(8,128)(2,1)S(1)} %convolution_convert_fusion.3), channel_id=1, source_target_pairs={{0,4},{4,1},{1,5},{5,2},{2,6},{6,3},{3,7},{8,12},{12,9},{9,13},{13... | collective-permute-start | bytes 1572872 | tf_op jit(solution)/shard_map/ppermute | solution.py:33
  222.9 25.6 %collective-permute-start.4 = (bf16[30,512]{1,0:T(8,128)(2,1)S(1)}, bf16[30,512]{1,0:T(8,128)(2,1)S(1)}, u32[]{:S(2)}, u32[]{:S(2)}) collective-permute-start(bf16[30,512]{1,0:T(8,128)(2,1)S(1)} %slice.268), channel_id=1, source_target_pairs={{0,4},{4,1},{1,5},{5,2},{2,6},{6,3},{3,7},{8,12},{12,9},{9,13},{13... | collective-permute-start | bytes 92168 | tf_op jit(solution)/shard_map/ppermute | solution.py:33
  231.0 12.2 %collective-permute-start.1 = (bf16[2,256,512]{2,1,0:T(8,128)(2,1)S(1)}, bf16[2,256,512]{2,1,0:T(8,128)(2,1)S(1)}, u32[]{:S(2)}, u32[]{:S(2)}) collective-permute-start(bf16[2,256,512]{2,1,0:T(8,128)(2,1)S(1)} %collective-permute-done), channel_id=1, source_target_pairs={{0,4},{4,1},{1,5},{5,2},{2,6},{6,3},{3,7},{8,12},{12,9},{9,13},{13... | collective-permute-start | bytes 1572872 | tf_op jit(solution)/shard_map/ppermute | solution.py:33
  241.8 13.8 %copy-start.16 = (f32[2]{0:T(128)S(1)}, f32[2]{0:T(128)}, u32[]{:S(2)}) copy-start(f32[2]{0:T(128)} %multiply_exponential_fusion.4) | copy-start | bytes 28
  241.8 13.8 %copy-start.17 = (f32[2]{0:T(128)S(1)}, f32[2]{0:T(128)}, u32[]{:S(2)}) copy-start(f32[2]{0:T(128)} %multiply_exponential_fusion.3) | copy-start | bytes 28
  244.0 11.5 %collective-permute-start.2 = (bf16[2,256,512]{2,1,0:T(8,128)(2,1)S(1)}, bf16[2,256,512]{2,1,0:T(8,128)(2,1)S(1)}, u32[]{:S(2)}, u32[]{:S(2)}) collective-permute-start(bf16[2,256,512]{2,1,0:T(8,128)(2,1)S(1)} %fusion.27), channel_id=1, source_target_pairs={{0,1},{4,5},{1,2},{5,6},{2,3},{6,7},{8,9},{12,13},{9,10},{13,14},{... | collective-permute-start | bytes 1572872 | tf_op jit(solution)/shard_map/ppermute | solution.py:33
  248.5 8.7 %copy-start.14 = (f32[512]{0:T(512)S(1)}, f32[512]{0:T(512)}, u32[]{:S(2)}) copy-start(f32[512]{0:T(512)} %dynamic_slice.10) | copy-start | bytes 6148
  248.5 8.7 %copy-start.15 = (f32[512]{0:T(512)S(1)}, f32[512]{0:T(512)}, u32[]{:S(2)}) copy-start(f32[512]{0:T(512)} %dynamic_slice.11) | copy-start | bytes 6148
  254.4 15.7 %copy-start = (f32[2,512,512]{2,1,0:T(8,128)S(1)}, f32[2,512,512]{2,1,0:T(8,128)}, u32[]{:S(2)}) copy-start(f32[2,512,512]{2,1,0:T(8,128)} %fusion.9) | copy-start | bytes 6291460
  254.4 15.6 %copy-start.18 = (f32[2]{0:T(128)S(1)}, f32[2]{0:T(128)}, u32[]{:S(2)}) copy-start(f32[2]{0:T(128)} %multiply_exponential_fusion.2) | copy-start | bytes 28
  255.9 14.1 %collective-permute-start.3 = (bf16[2,256,512]{2,1,0:T(8,128)(2,1)S(1)}, bf16[2,256,512]{2,1,0:T(8,128)(2,1)S(1)}, u32[]{:S(2)}, u32[]{:S(2)}) collective-permute-start(bf16[2,256,512]{2,1,0:T(8,128)(2,1)S(1)} %fusion.30), channel_id=1, source_target_pairs={{0,2},{4,6},{1,3},{5,7},{8,10},{12,14},{9,11},{13,15},{16,18},{20,... | collective-permute-start | bytes 1572872 | tf_op jit(solution)/shard_map/ppermute | solution.py:33
  273.4 2.6 copy-start.5
  336.2 27.8 %collective-permute-start.5 = (bf16[128,2048]{1,0:T(8,128)(2,1)}, bf16[128,2048]{1,0:T(8,128)(2,1)S(1)}, u32[]{:S(2)}, u32[]{:S(2)}) collective-permute-start(bf16[128,2048]{1,0:T(8,128)(2,1)} %reduce-scatter.2.cloned.1.call-done), channel_id=1, source_target_pairs={{0,0},{1,8},{2,16},{3,24},{8,1},{9,9},{10,17},{11,25},{16,2},{17,1... | collective-permute-start | bytes 1572872 | tf_op jit(solution)/shard_map/ppermute | solution.py:27
  (4 other events, 5.3 us)
Sparse Core Ops, SparseCore 0:
  283.6 52.6 reduce-scatter.1
where the time goes:
time: 373 us; the launch traced here: 372 us
  Pallas kernels  179 us (48%)
  waiting for transfers between devices  89.9 us (24%)
  matrix products  32.6 us (9%)
  other arithmetic  25.8 us (7%)
  starting transfers between devices  17.6 us (5%)
  between operations  13.8 us (4%)
  local copies, waits for them, and re-layouts  12.4 us (3%)
    pallas_call x1, Pallas kernels, spread(): pl.pallas_call(lambda *refs: spread_kernel(count, *refs), out_shape=outs,...  179 us
    reduce_scatter x1, waiting for transfers between devices, local(): lax.psum_scatter(mixed, 'hi', scatter_dimension=0, tiled=True)  52.8 us
    ppermute x1, waiting for transfers between devices, swap_planes(): return lax.ppermute(x, ('hi', 'tp'), pairs)  24.3 us
    dot_general x2, matrix products, project(): jnp.dot(rows, merged, preferred_element_type=jnp.float32)  19.4 us
    ppermute x5, starting transfers between devices, from_behind(): return lax.ppermute(x, ('lo', 'tp'), list(zip(spot[:-by], spot[by:])))  14 us
    ppermute x5, waiting for transfers between devices, from_behind(): return lax.ppermute(x, ('lo', 'tp'), list(zip(spot[:-by], spot[by:])))  12.8 us
  transfers between devices with their start and end apart: 7, of which 5 were waited for; matrix products, arithmetic and copies ran while one was open for 9% of the time, Pallas kernels for 0%

commit v1 on v0

v1 whole, which is shorter than its diff:
```python
import jax
import jax.numpy as jnp
from jax import lax
from jax.experimental import pallas as pl
from jax.experimental.pallas import tpu as pltpu
from jax.sharding import Mesh
from jax.sharding import PartitionSpec as P

KEY = 256
VAL = 512
GROUP = 512
KW = 31


rms_eps = 1e-06
group_eps = 1.0
layer_eps = 0.001
rope_base = 10000.0


SPANS = ("tp", "lo")


def swap_planes(x):
    size = lax.axis_size("tp")
    pairs = [(h * size + t, t * size + h) for h in range(size) for t in range(size)]
    return lax.ppermute(x, ("hi", "tp"), pairs)


def from_behind(x, by):
    outer, inner = lax.axis_size("tp"), lax.axis_size("lo")
    spot = [(i % inner) * outer + i // inner for i in range(outer * inner)]
    return lax.ppermute(x, ("lo", "tp"), list(zip(spot[:-by], spot[by:])))


def carried_in(contribution, log_span_decay):
    length = lax.axis_size(SPANS)
    state = from_behind(contribution.astype(jnp.bfloat16), 1).astype(jnp.float32)
    by = 1
    while by < length:
        earlier = from_behind(state.astype(jnp.bfloat16), by).astype(jnp.float32)
        state = state + jnp.exp(log_span_decay * by)[:, None, None] * earlier
        by *= 2
    return state


def rms_normalize(tokens, norm_gain):
    widened = tokens.astype(jnp.float32)
    scaled = widened * lax.rsqrt(jnp.mean(widened * widened, axis=-1, keepdims=True) + rms_eps)
    return (scaled * norm_gain).astype(jnp.bfloat16)


def rotate(vectors, positions):
    half_width = vectors.shape[-1] // 2
    frequency = rope_base ** (-jnp.arange(half_width, dtype=jnp.float32) / half_width)
    angles = positions.astype(jnp.float32)[:, None] * frequency
    cosine = jnp.cos(angles)[:, None, :]
    sine_part = jnp.sin(angles)[:, None, :]
    front_half = vectors[..., :half_width]
    back_half = vectors[..., half_width:]
    return jnp.concatenate(
        [front_half * cosine - back_half * sine_part, front_half * sine_part + back_half * cosine],
        axis=-1,
    )


def prepare(queries, key_rows, values, positions):
    row_count = queries.shape[0]
    rotated_query = rotate(
        queries.astype(jnp.float32).reshape(row_count, -1, KEY), positions
    ).astype(jnp.bfloat16)
    rotated_keys = (
        rotate(key_rows.astype(jnp.float32).reshape(row_count, -1, KEY), positions) * KEY ** (-0.5)
    ).astype(jnp.bfloat16)
    value_heads = values.reshape(row_count, -1, VAL)
    return (rotated_query, rotated_keys, value_heads)


def decay_logs(first_head, head_total, all_heads, seq_length):
    ratio = (first_head + jnp.arange(head_total)).astype(jnp.float32) / (all_heads - 1)
    return (jnp.log(0.05) + ratio * jnp.log(18.0)) / seq_length


def local_parts(queries, key_rows, values, log_decay):
    row_count = queries.shape[0]
    indices = jnp.arange(row_count, dtype=jnp.float32)
    offsets = indices[:, None] - indices[None, :]
    causal = offsets >= 0
    weight = jnp.where(
        causal[None], jnp.exp(log_decay[:, None, None] * jnp.where(causal, offsets, 0.0)[None]), 0.0
    )
    scores = (
        jnp.einsum("ihd,jhd->hij", queries, key_rows, preferred_element_type=jnp.float32) * weight
    ).astype(jnp.bfloat16)
    within = jnp.einsum("hij,jhe->ihe", scores, values, preferred_element_type=jnp.float32)
    trailing = jnp.exp(log_decay[None, :] * (row_count - 1.0 - indices)[:, None])
    weighted = (key_rows.astype(jnp.float32) * trailing[:, :, None]).astype(jnp.bfloat16)
    contribution = jnp.einsum("jhd,jhe->hde", weighted, values, preferred_element_type=jnp.float32)
    return (within, contribution)


def cross_part(queries, carry_state, log_decay):
    row_count = queries.shape[0]
    indices = jnp.arange(row_count, dtype=jnp.float32)
    leading = jnp.exp(log_decay[None, :] * (indices + 1.0)[:, None])
    return (
        jnp.einsum(
            "ihd,hde->ihe",
            queries,
            carry_state.astype(jnp.bfloat16),
            preferred_element_type=jnp.float32,
        )
        * leading[:, :, None]
    )


def retain_finish(raw, switch):
    average = jnp.mean(raw, axis=-1, keepdims=True)
    spread = jnp.mean(jnp.square(raw - average), axis=-1, keepdims=True)
    normalized = ((raw - average) * lax.rsqrt(spread + group_eps)).reshape(raw.shape[0], -1)
    return (normalized * jax.nn.silu(switch.astype(jnp.float32))).astype(jnp.bfloat16)


def convolve_branch(gated_input, before, tap_slice, gain_slice, shift_slice, switch):
    padded = jnp.concatenate([before, gated_input], axis=0)
    row_count = gated_input.shape[0]
    summed = jnp.zeros(gated_input.shape, jnp.float32)
    for tap_index in range(tap_slice.shape[0]):
        summed = (
            summed
            + padded[tap_index : tap_index + row_count].astype(jnp.float32) * tap_slice[tap_index]
        )
    grouped = summed.reshape(row_count, -1, GROUP)
    average = jnp.mean(grouped, axis=-1, keepdims=True)
    spread = jnp.mean(jnp.square(grouped - average), axis=-1, keepdims=True)
    normalized = ((grouped - average) * lax.rsqrt(spread + layer_eps)).reshape(row_count, -1)
    normalized = normalized * gain_slice + shift_slice
    return (jax.nn.silu(normalized) * jax.nn.silu(switch.astype(jnp.float32))).astype(jnp.bfloat16)


def contract(hidden, matrix):
    return lax.dot_general(
        hidden, matrix, (((1,), (1,)), ((), ())), preferred_element_type=jnp.float32
    )


def local(
    tokens,
    norm_gain,
    query_weight,
    key_weight,
    value_weight,
    retain_gate,
    unit_value,
    unit_gate,
    convolve_gate,
    filter_taps,
    layer_gain,
    layer_shift,
    retain_output,
    convolve_output,
):
    head_groups = lax.axis_size("hi")
    chain_length = lax.axis_size(SPANS)
    head_rank = lax.axis_index("hi")
    chain_rank = lax.axis_index(SPANS)
    def project(rows, merged, *matrices):
        product = jnp.dot(rows, merged, preferred_element_type=jnp.float32).astype(jnp.bfloat16)
        ends = [sum(m.shape[1] for m in matrices[: k + 1]) for k in range(len(matrices) - 1)]
        return jnp.split(product, ends, axis=1)

    first = (key_weight, value_weight, query_weight)
    second = (unit_value, unit_gate, convolve_gate, retain_gate)
    third = (retain_output, convolve_output)
    groups = (first, second, third)
    merged = [jnp.concatenate(group, axis=1) for group in groups]
    normed = rms_normalize(tokens, norm_gain)
    normed = lax.all_gather(swap_planes(normed), "hi", axis=0, tiled=True)
    merged = [lax.all_gather(swap_planes(m), SPANS, axis=0, tiled=True) for m in merged]
    key_rows, values, queries = project(normed, merged[0], *first)
    glu_value, glu_switch, convolve_switch, retain_switch = project(normed, merged[1], *second)
    out_full = merged[2]
    row_count = normed.shape[0]
    local_heads = queries.shape[1] // KEY
    positions = chain_rank * row_count + jnp.arange(row_count, dtype=jnp.int32)
    rotated_query, rotated_keys, value_heads = prepare(queries, key_rows, values, positions)
    log_decay = decay_logs(
        head_rank * local_heads, local_heads, local_heads * head_groups, row_count * chain_length
    )
    within, contribution = local_parts(rotated_query, rotated_keys, value_heads, log_decay)
    gated_input = (
        glu_value.astype(jnp.float32) * jax.nn.sigmoid(glu_switch.astype(jnp.float32))
    ).astype(jnp.bfloat16)
    channels = gated_input.shape[1]
    before = from_behind(gated_input[row_count - (KW - 1) :], 1)
    incoming = carried_in(contribution, log_decay * row_count)
    raw = within + cross_part(rotated_query, incoming, log_decay)
    retain_hidden = retain_finish(raw, retain_switch)
    tap_slice = lax.dynamic_slice_in_dim(filter_taps, head_rank * channels, channels, 1)
    gain_slice = lax.dynamic_slice_in_dim(layer_gain, head_rank * channels, channels, 0)
    shift_slice = lax.dynamic_slice_in_dim(layer_shift, head_rank * channels, channels, 0)
    convolve_hidden = convolve_branch(
        gated_input, before, tap_slice, gain_slice, shift_slice, convolve_switch
    )
    hidden = jnp.concatenate([retain_hidden, convolve_hidden], axis=1)
    mixed = contract(hidden, out_full).astype(jnp.bfloat16)
    return swap_planes(lax.psum_scatter(mixed, "hi", scatter_dimension=0, tiled=True))


UNITS_IN = 9
AHEAD = 3
MESH = pl.DeviceIdType.MESH
SQUARE = ("zh", "zl", "y", "x", "c")
CHAIN = ("c", "zl", "y")


def remote(source, target, out_sem, in_sem, device):
    return pltpu.make_async_remote_copy(
        src_ref=source,
        dst_ref=target,
        send_sem=out_sem,
        recv_sem=in_sem,
        device_id=device,
        device_id_type=MESH,
    )


def place():
    return tuple(lax.axis_index(name) for name in SQUARE)


class Gather:
    def __init__(self, source, full, near, send, arrive, beside):
        self.source, self.full, self.near = source, full, near
        self.send, self.arrive, self.beside = send, arrive, beside
        zh, zl, y, x, c = self.at = place()
        self.depth = source.shape[1]
        self.half = self.depth // 2
        self.outer = zl * zh + (1 - zl) * (1 - zh)
        self.mine = self.index(zh, self.outer, y)
        self.is_own = c == zh

    def index(self, zh, outer, y):
        zl = outer * zh + (1 - outer) * (1 - zh)
        return (zh * 2 + zl) * 2 + y

    def own(self, outer, flip):
        return self.index(self.at[0], outer, self.at[2] if not flip else 1 - self.at[2])

    def far(self, outer, flip):
        return self.index(1 - self.at[0], outer, self.at[2] if not flip else 1 - self.at[2])

    def rows(self, k, s, half):
        start = pl.multiple_of(s * self.depth + half * self.half, self.half)
        return self.full.at[k, pl.ds(start, self.half)]

    def whole(self, k, s):
        return self.full.at[k, pl.ds(pl.multiple_of(s * self.depth, self.depth), self.depth)]

    def z_mate(self, core):
        zh, zl, y, x, c = self.at
        return (zh, 1 - zl, y, x, core)

    def y_mate(self, core):
        zh, zl, y, x, c = self.at
        return (zh, zl, 1 - y, x, core)

    def sibling(self):
        zh, zl, y, x, c = self.at
        return (zh, zl, y, x, 1 - c)

    def load(self, k, ref, first):
        part = ref.at[:, pl.ds(first, self.source.shape[2])]

        @pl.when(self.is_own)
        def _():
            pltpu.make_async_copy(part, self.whole(k, self.mine), self.near.at[k]).start()

        @pl.when(jnp.logical_not(self.is_own))
        def _():
            pltpu.make_async_copy(part, self.source.at[k], self.near.at[k]).start()

    def own_sends(self, k):
        zh, zl, y, x, c = self.at
        part = self.whole(k, self.mine)
        copies = [remote(part, part, self.send.at[k, 16], self.beside.at[k], self.sibling())]
        for r in range(2):
            piece = self.rows(k, self.mine, r)
            arrive = self.arrive.at[k, self.mine, r]
            copies.append(remote(piece, piece, self.send.at[k, 12 + r], arrive, self.z_mate(r)))
            copies.append(remote(piece, piece, self.send.at[k, 14 + r], arrive, self.y_mate(r)))
        return copies

    def far_sends(self, k):
        zh, zl, y, x, c = self.at
        copies = []
        for r in range(2):
            piece = self.source.at[k, pl.ds(r * self.half, self.half)]
            copies.append(
                remote(
                    piece,
                    self.rows(k, self.mine, r),
                    self.send.at[k, 12 + r],
                    self.arrive.at[k, self.mine, r],
                    (c, 1 - c, y, x, r),
                )
            )
        return copies

    def begin(self, k):
        pltpu.make_async_copy(self.source.at[k], self.source.at[k], self.near.at[k]).wait()

        @pl.when(self.is_own)
        def _():
            for copy in self.own_sends(k):
                copy.start()

        @pl.when(jnp.logical_not(self.is_own))
        def _():
            for copy in self.far_sends(k):
                copy.start()

    def onward(self, k, s, device, slot):
        piece = self.rows(k, s, self.at[4])
        return remote(piece, piece, self.send.at[k, slot], self.arrive.at[k, s, self.at[4]], device)

    def landed(self, k, s, half):
        piece = self.rows(k, s, half)
        remote(
            piece, piece, self.send.at[k, 0], self.arrive.at[k, s, half], self.sibling()
        ).wait_recv()

    def table(self):
        c = self.at[4]
        z_mate, y_mate, sibling = self.z_mate(c), self.y_mate(c), self.sibling()
        inner = (
            (
                (self.far(0, 0), ((z_mate, 0, None), (y_mate, 1, None), (sibling, 2, None))),
                (self.far(1, 0), ((z_mate, 3, None), (y_mate, 4, None), (sibling, 5, None))),
                (self.own(0, 1), ((z_mate, 8, 0), (sibling, 7, None))),
                (self.own(1, 0), ((sibling, 6, None),)),
            ),
            (
                (self.far(0, 1), ((sibling, 9, None),)),
                (self.far(1, 1), ((sibling, 10, None),)),
                (self.own(1, 1), ((sibling, 11, None),)),
            ),
            (),
        )
        outer = (
            (
                (self.own(1, 1), ((z_mate, 2, None), (sibling, 3, None))),
                (self.own(0, 0), ((y_mate, 1, 1), (sibling, 0, None))),
            ),
            (
                (self.far(0, 0), ((y_mate, 4, None), (sibling, 5, None))),
                (self.far(1, 0), ((y_mate, 6, None), (sibling, 7, None))),
            ),
            (
                (self.own(0, 1), ((sibling, 10, None),)),
                (self.far(0, 1), ((sibling, 8, None),)),
                (self.far(1, 1), ((sibling, 9, None),)),
            ),
        )
        return inner, outer

    def stage(self, k, number):
        for role, moves in enumerate(self.table()):
            if not moves[number]:
                continue

            @pl.when(self.outer == role)
            def _():
                for s, targets in moves[number]:
                    self.landed(k, s, self.at[4])
                    for device, slot, lane in targets:
                        copy = self.onward(k, s, device, slot)
                        if lane is None:
                            copy.start()
                        else:
                            pl.when(self.at[4] == lane)(copy.start)

    def complete(self, k):
        other = 1 - self.at[4]
        for s in (
            self.own(1 - self.outer, 0),
            self.own(self.outer, 1),
            self.own(1 - self.outer, 1),
            self.far(0, 0),
            self.far(1, 0),
            self.far(0, 1),
            self.far(1, 1),
        ):
            self.landed(k, s, other)

        @pl.when(jnp.logical_not(self.is_own))
        def _():
            part = self.whole(k, self.mine)
            remote(
                part, part, self.send.at[k, 0], self.beside.at[k], self.sibling()
            ).wait_recv()

    def drain(self, k):
        @pl.when(self.is_own)
        def _():
            for copy in self.own_sends(k):
                copy.wait_send()

        @pl.when(jnp.logical_not(self.is_own))
        def _():
            for copy in self.far_sends(k):
                copy.wait_send()

        for role, moves in enumerate(self.table()):

            @pl.when(self.outer == role)
            def _():
                for number in range(3):
                    for s, targets in moves[number]:
                        for device, slot, lane in targets:
                            copy = self.onward(k, s, device, slot)
                            if lane is None:
                                copy.wait_send()
                            else:
                                pl.when(self.at[4] == lane)(copy.wait_send)


def gather_scratch(units, depth, width, shares, dtype):
    return [
        pltpu.VMEM((units, depth, width), dtype),
        pltpu.VMEM((units, shares * depth, width), dtype),
        pltpu.SemaphoreType.DMA((units,)),
        pltpu.SemaphoreType.DMA((units, 17)),
        pltpu.SemaphoreType.DMA((units, shares, 2)),
        pltpu.SemaphoreType.DMA((units,)),
    ]


def gather_kernel(layout, units, *refs):
    rows_ref, blocks = refs[0], refs[1:10]
    product_ref, out_ref = refs[10:12]
    normed = refs[12]
    source, full, near, send, arrive, beside = refs[13:19]
    rows_send, rows_arrive, out_sem = refs[19:]
    zh, zl, y, x, c = place()
    gather = Gather(source, full, near, send, arrive, beside)
    count = rows_ref.shape[0]
    mine = normed.at[pl.ds(pl.multiple_of((x * 2 + c) * count, count), count)]

    def rows_copy(dz, dx):
        to_z = zh if not dz else 1 - zh
        to_x = x if not dx else 1 - x
        return remote(
            rows_ref,
            mine,
            rows_send.at[dz * 2 + dx],
            rows_arrive.at[x * 2 + c],
            (to_z, zl, y, to_x, zh),
        )

    far_rows = ((0, 1), (1, 0), (1, 1))
    for dz, dx in far_rows:
        rows_copy(dz, dx).start()

    @pl.when(c == zh)
    def _():
        pltpu.make_async_copy(rows_ref, mine, rows_arrive.at[x * 2 + c]).start()

    @pl.when(c != zh)
    def _():
        rows_copy(0, 0).start()

    for k, (which, first) in enumerate(layout):
        gather.load(k, blocks[which], first)

    for k in range(AHEAD):
        gather.begin(k)

    for j in range(4):
        part = normed.at[pl.ds(j * count, count)]
        remote(part, part, rows_send.at[0], rows_arrive.at[j], gather.sibling()).wait_recv()

    def when_unit(k, limit, what):
        @pl.when(jnp.logical_and(k >= 0, k < limit))
        def _():
            what(k)

    def project(k):
        wide = full.shape[2] // 2
        for part in range(2):
            columns = pl.ds(part * wide, wide)
            product_ref[k, :, columns] = jnp.dot(
                normed[...], full[k, :, columns], preferred_element_type=jnp.float32
            ).astype(product_ref.dtype)

    def write_out(k):
        pltpu.make_async_copy(full.at[k], out_ref.at[k - UNITS_IN], out_sem.at[k - UNITS_IN]).start()

    def step(i, carry):
        when_unit(i, units, lambda k: gather.stage(k, 0))
        when_unit(i - 1, units, lambda k: gather.stage(k, 1))
        when_unit(i - 2, units, lambda k: gather.stage(k, 2))
        when_unit(i + AHEAD, units, gather.begin)
        when_unit(i - 3, units, gather.complete)
        when_unit(i - 3, UNITS_IN, project)

        @pl.when(i - 3 >= UNITS_IN)
        def _():
            write_out(i - 3)

        return carry

    lax.fori_loop(0, units + 3, step, 0)

    def finish(k, carry):
        gather.drain(k)
        return carry

    lax.fori_loop(0, units, finish, 0)
    for dz, dx in far_rows:
        rows_copy(dz, dx).wait_send()

    @pl.when(c != zh)
    def _():
        rows_copy(0, 0).wait_send()

    for k in range(units - UNITS_IN):
        pltpu.make_async_copy(full.at[UNITS_IN + k], out_ref.at[k], out_sem.at[k]).wait()


def gather_and_project(rows, blocks, width):
    layout = [(n, first) for n, b in enumerate(blocks) for first in range(0, b.shape[1], width)]
    units = len(layout)
    depth, shares, dtype = blocks[0].shape[0], 8, rows.dtype
    span = 4 * rows.shape[0]
    return pl.pallas_call(
        lambda *refs: gather_kernel(layout, units, *refs),
        out_shape=[
            jax.ShapeDtypeStruct((UNITS_IN, span, width), dtype),
            jax.ShapeDtypeStruct((units - UNITS_IN, shares * depth, width), dtype),
        ],
        in_specs=[pl.BlockSpec(memory_space=pl.ANY)] * (1 + len(blocks)),
        out_specs=[pl.BlockSpec(memory_space=pltpu.VMEM), pl.BlockSpec(memory_space=pl.ANY)],
        scratch_shapes=[pltpu.VMEM((span, rows.shape[1]), dtype)]
        + gather_scratch(units, depth, width, shares, dtype)
        + [
            pltpu.SemaphoreType.DMA((4,)),
            pltpu.SemaphoreType.DMA((4,)),
            pltpu.SemaphoreType.DMA((units - UNITS_IN,)),
        ],
        compiler_params=pltpu.CompilerParams(has_side_effects=True, vmem_limit_bytes=56 << 20),
        name="gather_project",
    )(rows, *blocks)


def finish_kernel(tile, first, second, third, matrix, out, kept, sent, got, half, here, there, sems):
    hidden = (first, second, third)
    zh, zl, y, x, c = place()
    tiles = matrix.shape[1] // tile
    share = out.shape[0]
    pair = 2 * share
    to_x, from_x, to_near, from_near, to_far, from_far = (sems.at[k] for k in range(6))
    across, sibling = (zh, zl, y, 1 - x, c), (zh, zl, y, x, 1 - c)
    stays = c == zh

    def x_copy(n):
        return remote(sent.at[n], got.at[n], to_x.at[n], from_x.at[n], across)

    def near_copy(n):
        part = half.at[n, pl.ds(pl.multiple_of((1 - c) * share, share), share)]
        return remote(part, here.at[n], to_near.at[n], from_near.at[n], sibling)

    def far_copy(n, core):
        part = half.at[n, pl.ds(core * share, share)]
        out_sem = (to_near if core == 0 else to_far).at[n]
        return remote(part, there.at[n], out_sem, from_far.at[n], (c, zl, y, x, core))

    def multiply(n):
        lines = pl.ds(pl.multiple_of(n * tile, tile), tile)
        total = contract(hidden[0][...], matrix[0, lines])
        total += contract(hidden[1][...], matrix[1, lines])
        total += contract(hidden[2][...], matrix[2, lines])
        low, high = total[:pair], total[pair:]
        kept[n] = jnp.where(x == 0, low, high)
        sent[n] = jnp.where(x == 0, high, low).astype(sent.dtype)
        x_copy(n).start()

    def join(n):
        x_copy(n).wait_recv()
        half[n] = (kept[n] + got[n].astype(jnp.float32)).astype(half.dtype)

        @pl.when(stays)
        def _():
            near_copy(n).start()

        @pl.when(jnp.logical_not(stays))
        def _():
            far_copy(n, 0).start()
            far_copy(n, 1).start()

    def close(n):
        remote(there.at[n], there.at[n], to_far.at[n], from_far.at[n], across).wait_recv()
        lines = pl.ds(pl.multiple_of(n * tile, tile), tile)
        far_part = there[n].astype(jnp.float32)

        @pl.when(stays)
        def _():
            mine = half[n, pl.ds(pl.multiple_of(c * share, share), share)].astype(jnp.float32)
            out[:, lines] = (mine + far_part).astype(out.dtype)

        @pl.when(jnp.logical_not(stays))
        def _():
            near_copy(n).wait_recv()
            out[:, lines] = (here[n].astype(jnp.float32) + far_part).astype(out.dtype)

    def when_tile(n, what):
        @pl.when(jnp.logical_and(n >= 0, n < tiles))
        def _():
            what(n)

    def step(i, carry):
        when_tile(i, multiply)
        when_tile(i - 3, join)
        when_tile(i - 6, close)
        return carry

    lax.fori_loop(0, tiles + 6, step, 0)

    def drain(n, carry):
        x_copy(n).wait_send()

        @pl.when(stays)
        def _():
            near_copy(n).wait_send()

        @pl.when(jnp.logical_not(stays))
        def _():
            far_copy(n, 0).wait_send()
            far_copy(n, 1).wait_send()

        return carry

    lax.fori_loop(0, tiles, drain, 0)


def finish_outputs(hidden, matrix, tile):
    span = hidden[0].shape[0]
    share = span // 4
    tiles = matrix.shape[1] // tile
    dtype = matrix.dtype
    return pl.pallas_call(
        lambda *refs: finish_kernel(tile, *refs),
        out_shape=jax.ShapeDtypeStruct((share, matrix.shape[1]), dtype),
        in_specs=[pl.BlockSpec(memory_space=pltpu.VMEM)] * 4,
        out_specs=pl.BlockSpec(memory_space=pltpu.VMEM),
        scratch_shapes=[
            pltpu.VMEM((tiles, 2 * share, tile), jnp.float32),
            pltpu.VMEM((tiles, 2 * share, tile), dtype),
            pltpu.VMEM((tiles, 2 * share, tile), dtype),
            pltpu.VMEM((tiles, 2 * share, tile), dtype),
            pltpu.VMEM((tiles, share, tile), dtype),
            pltpu.VMEM((tiles, share, tile), dtype),
            pltpu.SemaphoreType.DMA((6, tiles)),
        ],
        compiler_params=pltpu.CompilerParams(has_side_effects=True, vmem_limit_bytes=56 << 20),
        name="finish",
    )(*hidden, matrix)


def shifted(x, by):
    length, cores = lax.axis_size(CHAIN), lax.axis_size("c")
    inner = length // cores
    spot = [(i % inner) * cores + i // inner for i in range(length)]
    return lax.ppermute(x, ("zl", "y", "c"), list(zip(spot[:-by], spot[by:])))


def local_squares(
    tokens,
    norm_gain,
    query_weight,
    key_weight,
    value_weight,
    retain_gate,
    unit_value,
    unit_gate,
    convolve_gate,
    filter_taps,
    layer_gain,
    layer_shift,
    retain_output,
    convolve_output,
):
    rank = lax.axis_index("x") * 2 + lax.axis_index("zh")
    groups = 4
    chain_length = lax.axis_size(CHAIN)
    chain_rank = lax.axis_index(CHAIN)
    normed = rms_normalize(tokens, norm_gain)
    blocks = (key_weight, value_weight, query_weight, unit_value, unit_gate, convolve_gate)
    blocks += (retain_gate, retain_output, convolve_output)
    products, matrix = gather_and_project(normed, blocks, key_weight.shape[1])
    keys, value_0, value_1, queries, glu_value, glu_switch, convolve_switch, gate_0, gate_1 = (
        products[k] for k in range(UNITS_IN)
    )
    row_count = keys.shape[0]
    local_heads = 2
    positions = chain_rank * row_count + jnp.arange(row_count, dtype=jnp.int32)
    log_decay = decay_logs(
        rank * local_heads, local_heads, local_heads * groups, row_count * chain_length
    )
    values = jnp.concatenate([value_0, value_1], axis=1)
    rotated_query, rotated_keys, value_heads = prepare(queries, keys, values, positions)
    within, contribution = local_parts(rotated_query, rotated_keys, value_heads, log_decay)
    gated_input = (
        glu_value.astype(jnp.float32) * jax.nn.sigmoid(glu_switch.astype(jnp.float32))
    ).astype(jnp.bfloat16)
    channels = gated_input.shape[1]
    before = shifted(gated_input[row_count - (KW - 1) :], 1)
    log_span = log_decay * row_count
    state = shifted(contribution.astype(jnp.bfloat16), 1).astype(jnp.float32)
    by = 1
    while by < chain_length:
        earlier = shifted(state.astype(jnp.bfloat16), by).astype(jnp.float32)
        state = state + jnp.exp(log_span * by)[:, None, None] * earlier
        by *= 2
    raw = within + cross_part(rotated_query, state, log_decay)
    retain_hidden = retain_finish(raw, jnp.concatenate([gate_0, gate_1], axis=1))
    tap_slice = lax.dynamic_slice_in_dim(filter_taps, rank * channels, channels, 1)
    gain_slice = lax.dynamic_slice_in_dim(layer_gain, rank * channels, channels, 0)
    shift_slice = lax.dynamic_slice_in_dim(layer_shift, rank * channels, channels, 0)
    convolve_hidden = convolve_branch(
        gated_input, before, tap_slice, gain_slice, shift_slice, convolve_switch
    )
    hidden = (retain_hidden[:, :VAL], retain_hidden[:, VAL:], convolve_hidden)
    return finish_outputs(hidden, matrix, 256)


def squares(mesh):
    boxes = Mesh(mesh.devices.reshape(2, 2, 2, 2, 2), SQUARE)
    rows, blocks = P(SQUARE, None), P(("zh", "zl", "y"), ("x", "c"))
    return jax.shard_map(
        local_squares,
        mesh=boxes,
        in_specs=(rows, P()) + (blocks,) * 7 + (P(),) * 3 + (blocks,) * 2,
        out_specs=rows,
        check_vma=False,
    )


def solution(mesh):
    sp, tp = mesh.shape["sp"], mesh.shape["tp"]
    if (sp, tp) == (8, 4):
        return squares(mesh)
    planes = Mesh(mesh.devices.reshape(tp, sp // tp, tp), ("hi", "lo", "tp"))
    return jax.shard_map(
        local,
        mesh=planes,
        in_specs=(
            P(("hi", "lo", "tp"), None),
            P(),
            P(("hi", "lo"), "tp"),
            P(("hi", "lo"), "tp"),
            P(("hi", "lo"), "tp"),
            P(("hi", "lo"), "tp"),
            P(("hi", "lo"), "tp"),
            P(("hi", "lo"), "tp"),
            P(("hi", "lo"), "tp"),
            P(),
            P(),
            P(),
            P(("hi", "lo"), "tp"),
            P(("hi", "lo"), "tp"),
        ),
        out_specs=P(("hi", "lo", "tp"), None),
        check_vma=False,
    )
```

time: 373 us -> 316 us (0.85)
  the two profiles are of different devices: /device:TPU:2 before, /device:TPU:9 now
where the time goes in v1:
time: 316 us; the launch traced here: 312 us
  Pallas kernels  222 us (70%)
  other arithmetic  40.4 us (13%)
  waiting for transfers between devices  21.3 us (7%)
  local copies, waits for them, and re-layouts  13.1 us (4%)
  starting transfers between devices  9.69 us (3%)
  matrix products  4.88 us (2%)
    pallas_call x1, Pallas kernels, gather_and_project(): pl.pallas_call(lambda *refs: gather_kernel(layout, units, *refs), out_sha...  180 us
    pallas_call x1, Pallas kernels, finish_outputs(): pl.pallas_call(lambda *refs: finish_kernel(tile, *refs), out_shape=jax.Sh...  42.6 us
    ppermute x5, waiting for transfers between devices, shifted(): return lax.ppermute(x, ('zl', 'y', 'c'), list(zip(spot[:-by], spot[by:])))  21.3 us
    reduce_sum x1, other arithmetic, convolve_branch(): average = jnp.mean(grouped, axis=-1, keepdims=True)  17.6 us
    ppermute x5, starting transfers between devices, shifted(): return lax.ppermute(x, ('zl', 'y', 'c'), list(zip(spot[:-by], spot[by:])))  9.69 us
  transfers between devices with their start and end apart: 5, of which 3 were waited for; matrix products, arithmetic and copies ran while one was open for 14% of the time, Pallas kernels for 0%

profile of v1, /device:TPU:9, one launch (start us, length us, event | category | flops | bytes accessed | tf_op | source)
XLA Modules:
  0.0 312.3 jit_solution(2332931674411755004)
XLA Ops:
  0.0 1.2 fusion.7
  1.2 2.0 fusion.9.refs_0_
  3.3 179.8 %gather_project.1 = (bf16[9,512,512]{2,1,0:T(8,128)(2,1)}, bf16[3,2048,512]{2,1,0:T(8,128)(2,1)}) custom-call(bf16[128,2048]{1,0:T(8,128)(2,1)} %fusion.9.refs_0_, bf16[256,512]{1,0:T(8,128)(2,1)} %refs_1_.1, bf16[256,1024]{1,0:T(8,128)(2,1)} %refs_2_.1, bf16[256,512]{1,0:T(8,128)(2,1)} %refs_3_.1, bf16[256,512]{1,0:T(8,128)(2,1)} %refs_4_.1, ...), custom_call_target="tpu_custom_call" | custom-call | tf_op jit(solution)/shard_map/gather_project/pallas_call | solution.py:536
  183.1 1.5 multiply_convert_fusion.1
  184.6 3.1 collective-permute-start.4
  187.8 3.4 %slice_bitcast_fusion.1 = (bf16[512,512]{1,0:T(8,128)(2,1)}, bf16[512,512]{1,0:T(8,128)(2,1)}, f32[1,512,512]{2,1,0:T(8,128)S(1)}, f32[1,512,512]{2,1,0:T(8,128)...) fusion(bf16[9,512,512]{2,1,0:T(8,128)(2,1)} %get-tuple-element.7), kind=kLoop, calls=%fused_computation.111 | loop fusion | flops 524288 | bytes 7340032 | tf_op jit(solution)/shard_map/squeeze | solution.py:702
  196.4 1.9 collective-permute-start
  198.9 1.2 fusion.75
  200.6 1.9 constant_dynamic-slice_fusion
  203.5 2.3 fusion.77
  205.8 14.3 %collective-permute-done = bf16[2,256,512]{2,1,0:T(8,128)(2,1)S(1)} collective-permute-done((bf16[2,256,512]{2,1,0:T(8,128)(2,1)S(1)}, bf16[2,256,512]{2,1,0:T(8,128)(2,1)S(1)}, u32[]{:S(2)}, u32[]{:S(2)}) %collective-permute-start) | collective-permute-done | bytes 524320 | tf_op jit(solution)/shard_map/ppermute | solution.py:674
  220.1 1.9 collective-permute-start.1
  222.5 1.3 dynamic_slice.10
  223.9 1.3 dynamic_slice.11
  226.4 3.3 %fusion.6 = f32[2,512,512]{2,1,0:T(8,128)S(1)} fusion(f32[512,512]{1,0:T(8,128)} %fusion.18, f32[2]{0:T(128)} %copy-done.12, pred[512,512]{1,0:T(8,128)(4,1)} %fusion.19, bf16[512,1,512]{2,0,1:T(8,128)(2,1)} %get-tuple-element.15, bf16[512,1,512]{2,0,1:T(8,128)(2,1)} %get-tuple-element.16, bf16[512,2,128]{2,0,1:T(8,128)(2,1)S(1)} %get-tuple-element.27, ...), kind=kOutput, calls=%fused_computation.41 | convolution fusion | flops 809762816 | bytes 6029320 | tf_op jit(solution)/shard_map/hij,jhe->ihe/dot_general | solution.py:95
  229.7 6.2 %collective-permute-done.1 = bf16[2,256,512]{2,1,0:T(8,128)(2,1)S(1)} collective-permute-done((bf16[2,256,512]{2,1,0:T(8,128)(2,1)S(1)}, bf16[2,256,512]{2,1,0:T(8,128)(2,1)S(1)}, u32[]{:S(2)}, u32[]{:S(2)}) %collective-permute-start.1) | collective-permute-done | bytes 524320 | tf_op jit(solution)/shard_map/ppermute | solution.py:674
  236.8 1.5 collective-permute-start.2
  238.3 17.6 %fusion.71 = (f32[512]{0:T(512)S(1)}, f32[512,512]{1,0:T(8,128)S(1)}) fusion(f32[512]{0:T(512)S(1)} %bitcast.66, bf16[512,512]{1,0:T(8,128)(2,1)} %fusion.77, f32[512]{0:T(512)S(1)} %bitcast.68, bf16[30,512]{1,0:T(8,128)(2,1)S(1)} %collective-permute-done.4, f32[512]{0:T(512)S(1)} %bitcast.69, f32[512]{0:T(512)S(1)} %bitcast.70, f32[512]{0:T(512)S(1)} %bitcast.71, ...), kind=kLoop, calls=%fused_computation.152 | loop fusion | flops 47971840 | bytes 1669120 | tf_op jit(solution)/shard_map/reduce_sum | solution.py:134
  256.6 1.3 collective-permute-start.3
  258.0 2.5 fusion.20.refs_2_
  262.4 1.6 subtract_multiply_fusion
  264.1 2.0 copy.26
  267.8 42.6 %finish.1 = bf16[128,2048]{1,0:T(8,128)(2,1)} custom-call(bf16[512,512]{1,0:T(8,128)(2,1)} %get-tuple-element.22.refs_0_, bf16[512,512]{1,0:T(8,128)(2,1)} %get-tuple-element.21.refs_1_, bf16[512,512]{1,0:T(8,128)(2,1)} %fusion.20.refs_2_, bf16[3,2048,512]{2,1,0:T(8,128)(2,1)} %get-tuple-element.8.refs_3_), custom_call_target="tpu_custom_call" | custom-call | tf_op jit(solution)/shard_map/finish/pallas_call | solution.py:651
  310.4 1.9 copy.40
  (58 shorter events, 14.1 us)
Async XLA Ops:
  184.6 53.6 %collective-permute-start.4 = (bf16[30,512]{1,0:T(8,128)(2,1)S(1)}, bf16[30,512]{1,0:T(8,128)(2,1)S(1)}, u32[]{:S(2)}, u32[]{:S(2)}) collective-permute-start(bf16[30,512]{1,0:T(8,128)(2,1)S(1)} %slice_bitcast_fusion.4), channel_id=1, source_target_pairs={{0,4},{4,8},{8,12},{12,1},{1,5},{5,9},{9,13},{2,6},{6,10},{10,14},... | collective-permute-start | bytes 92168 | tf_op jit(solution)/shard_map/ppermute | solution.py:674
  192.6 1.7 copy-start.12
  194.4 1.0 copy-start.3
  194.4 1.2 copy-start.4
  195.4 0.9 copy-start.5
  195.4 1.0 copy-start.6
  196.4 23.7 %collective-permute-start = (bf16[2,256,512]{2,1,0:T(8,128)(2,1)S(1)}, bf16[2,256,512]{2,1,0:T(8,128)(2,1)S(1)}, u32[]{:S(2)}, u32[]{:S(2)}) collective-permute-start(bf16[2,256,512]{2,1,0:T(8,128)(2,1)S(1)} %convolution_convert_fusion), channel_id=1, source_target_pairs={{0,4},{4,8},{8,12},{12,1},{1,5},{5,9},{9,13},{2,6},{6,10},{10,14},... | collective-permute-start | bytes 1572872 | tf_op jit(solution)/shard_map/ppermute | solution.py:674
  220.1 15.8 %collective-permute-start.1 = (bf16[2,256,512]{2,1,0:T(8,128)(2,1)S(1)}, bf16[2,256,512]{2,1,0:T(8,128)(2,1)S(1)}, u32[]{:S(2)}, u32[]{:S(2)}) collective-permute-start(bf16[2,256,512]{2,1,0:T(8,128)(2,1)S(1)} %collective-permute-done), channel_id=1, source_target_pairs={{0,4},{4,8},{8,12},{12,1},{1,5},{5,9},{9,13},{2,6},{6,10},{10,14},... | collective-permute-start | bytes 1572872 | tf_op jit(solution)/shard_map/ppermute | solution.py:674
  229.7 26.5 %copy-start.9 = (f32[2]{0:T(128)S(1)}, f32[2]{0:T(128)}, u32[]{:S(2)}) copy-start(f32[2]{0:T(128)} %multiply_exponential_fusion.4) | copy-start | bytes 28
  229.7 26.5 %copy-start.10 = (f32[2]{0:T(128)S(1)}, f32[2]{0:T(128)}, u32[]{:S(2)}) copy-start(f32[2]{0:T(128)} %multiply_exponential_fusion.3) | copy-start | bytes 28
  236.8 19.4 %collective-permute-start.2 = (bf16[2,256,512]{2,1,0:T(8,128)(2,1)S(1)}, bf16[2,256,512]{2,1,0:T(8,128)(2,1)S(1)}, u32[]{:S(2)}, u32[]{:S(2)}) collective-permute-start(bf16[2,256,512]{2,1,0:T(8,128)(2,1)S(1)} %fusion.22), channel_id=1, source_target_pairs={{0,8},{4,12},{8,1},{12,5},{1,9},{5,13},{2,10},{6,14},{10,3},{14,7}... | collective-permute-start | bytes 1572872 | tf_op jit(solution)/shard_map/ppermute | solution.py:674
  238.3 19.7 %copy-start.7 = (f32[512]{0:T(512)S(1)}, f32[512]{0:T(512)}, u32[]{:S(2)}) copy-start(f32[512]{0:T(512)} %dynamic_slice.10) | copy-start | bytes 6148
  238.3 19.7 %copy-start.8 = (f32[512]{0:T(512)S(1)}, f32[512]{0:T(512)}, u32[]{:S(2)}) copy-start(f32[512]{0:T(512)} %dynamic_slice.11) | copy-start | bytes 6148
  256.2 5.0 %copy-start.2 = (bf16[512,2,128]{2,0,1:T(8,128)(2,1)S(1)}, bf16[512,2,128]{2,0,1:T(8,128)(2,1)}, u32[]{:S(2)}) copy-start(bf16[512,2,128]{2,0,1:T(8,128)(2,1)} %get-tuple-element.28) | copy-start | bytes 786436
  256.2 5.0 %copy-start.11 = (f32[2]{0:T(128)S(1)}, f32[2]{0:T(128)}, u32[]{:S(2)}) copy-start(f32[2]{0:T(128)} %multiply_exponential_fusion.2) | copy-start | bytes 28
  256.6 4.6 %collective-permute-start.3 = (bf16[2,256,512]{2,1,0:T(8,128)(2,1)S(1)}, bf16[2,256,512]{2,1,0:T(8,128)(2,1)S(1)}, u32[]{:S(2)}, u32[]{:S(2)}) collective-permute-start(bf16[2,256,512]{2,1,0:T(8,128)(2,1)S(1)} %fusion.23), channel_id=1, source_target_pairs={{0,1},{4,5},{8,9},{12,13},{2,3},{6,7},{10,11},{14,15},{16,17},{20,... | collective-permute-start | bytes 1572872 | tf_op jit(solution)/shard_map/ppermute | solution.py:674
  264.1 2.0 copy-start
  264.1 2.0 copy-start.1

commit v2 on v1

--- a/solution.py
+++ b/solution.py
@@ -1,3 +1,5 @@
+import math
+
 import jax
 import jax.numpy as jnp
 from jax import lax
@@ -207,8 +209,10 @@
     return swap_planes(lax.psum_scatter(mixed, "hi", scatter_dimension=0, tiled=True))
 
 
-UNITS_IN = 9
-AHEAD = 3
+AHEAD = 5
+LAGS = (0, 2, 3, 4)
+ROWS_AFTER = 2
+ROWS_RELAY = 3
 MESH = pl.DeviceIdType.MESH
 SQUARE = ("zh", "zl", "y", "x", "c")
 CHAIN = ("c", "zl", "y")
@@ -269,16 +273,18 @@
         zh, zl, y, x, c = self.at
         return (zh, zl, y, x, 1 - c)
 
-    def load(self, k, ref, first):
-        part = ref.at[:, pl.ds(first, self.source.shape[2])]
+    def load(self, k, part, columns):
+        columns = pl.ds(0, self.source.shape[2]) if columns is None else columns
 
         @pl.when(self.is_own)
         def _():
-            pltpu.make_async_copy(part, self.whole(k, self.mine), self.near.at[k]).start()
+            target = self.whole(k, self.mine).at[:, columns]
+            pltpu.make_async_copy(part, target, self.near.at[k]).start()
 
         @pl.when(jnp.logical_not(self.is_own))
         def _():
-            pltpu.make_async_copy(part, self.source.at[k], self.near.at[k]).start()
+            target = self.source.at[k].at[:, columns]
+            pltpu.make_async_copy(part, target, self.near.at[k]).start()
 
     def own_sends(self, k):
         zh, zl, y, x, c = self.at
@@ -436,242 +442,638 @@
     ]
 
 
-def gather_kernel(layout, units, *refs):
-    rows_ref, blocks = refs[0], refs[1:10]
-    product_ref, out_ref = refs[10:12]
-    normed = refs[12]
-    source, full, near, send, arrive, beside = refs[13:19]
-    rows_send, rows_arrive, out_sem = refs[19:]
-    zh, zl, y, x, c = place()
-    gather = Gather(source, full, near, send, arrive, beside)
-    count = rows_ref.shape[0]
-    mine = normed.at[pl.ds(pl.multiple_of((x * 2 + c) * count, count), count)]
-
-    def rows_copy(dz, dx):
-        to_z = zh if not dz else 1 - zh
-        to_x = x if not dx else 1 - x
+class Layer:
+    def __init__(self, refs):
+        names = (
+            "rows",
+            "cosine",
+            "sine",
+            "taps",
+            "gain",
+            "shift",
+            "out",
+            "normed",
+            "products",
+            "keys",
+            "queries",
+            "within",
+            "sending",
+            "got",
+            "prefix",
+            "state",
+            "padded",
+            "halo_out",
+            "halo_in",
+            "summed",
+            "hidden",
+            "kept",
+            "sent",
+            "crossed",
+            "half",
+            "here",
+            "there",
+        )
+        for name, ref in zip(names, refs):
+            setattr(self, name, ref)
+        sems = refs[len(names) :]
+        (
+            self.rows_send,
+            self.rows_arrive,
+            self.slice_sems,
+            self.prefix_sems,
+            self.halo_sems,
+            self.out_sems,
+        ) = sems
+        zh, zl, y, x, c = self.at = place()
+        self.count = self.normed.shape[0]
+        self.heads = self.keys.shape[1] // KEY
+        self.rank = x * 2 + zh
+        self.link = (c * 2 + zl) * 2 + y
+        self.links = 8
+        self.groups = 4
+
+    def chain(self, s):
+        zh, zl, y, x, c = self.at
+        return (zh, (s // 2) % 2, s % 2, x, s // 4)
+
+    def log_decay(self, head):
+        ratio = (self.rank * self.heads + head).astype(jnp.float32) / (
+            self.heads * self.groups - 1
+        )
+        return (math.log(0.05) + ratio * math.log(18.0)) / (self.count * self.links)
+
+    def by_rows(self, size, what):
+        def body(n, carry):
+            what(pl.multiple_of(n * size, size))
+            return carry
+
+        lax.fori_loop(0, self.count // size, body, 0)
+
+    def position(self, first, size):
+        rows = lax.broadcasted_iota(jnp.int32, (size, 1), 0) + first
+        return rows.astype(jnp.float32)
+
+
+    def block(self, j):
+        share = self.rows.shape[0]
+        return self.normed.at[pl.ds(pl.multiple_of(j * share, share), share)]
+
+    def rows_copy(self, dz, dx):
+        zh, zl, y, x, c = self.at
+        j = x * 2 + c
+        to = (1 - zh if dz else zh, zl, y, 1 - x if dx else x, zh)
         return remote(
-            rows_ref,
-            mine,
-            rows_send.at[dz * 2 + dx],
-            rows_arrive.at[x * 2 + c],
-            (to_z, zl, y, to_x, zh),
-        )
-
-    far_rows = ((0, 1), (1, 0), (1, 1))
-    for dz, dx in far_rows:
-        rows_copy(dz, dx).start()
-
-    @pl.when(c == zh)
-    def _():
-        pltpu.make_async_copy(rows_ref, mine, rows_arrive.at[x * 2 + c]).start()
-
-    @pl.when(c != zh)
-    def _():
-        rows_copy(0, 0).start()
-
-    for k, (which, first) in enumerate(layout):
-        gather.load(k, blocks[which], first)
-
-    for k in range(AHEAD):
-        gather.begin(k)
-
-    for j in range(4):
-        part = normed.at[pl.ds(j * count, count)]
-        remote(part, part, rows_send.at[0], rows_arrive.at[j], gather.sibling()).wait_recv()
-
-    def when_unit(k, limit, what):
-        @pl.when(jnp.logical_and(k >= 0, k < limit))
-        def _():
-            what(k)
-
-    def project(k):
-        wide = full.shape[2] // 2
+            self.rows, self.block(j), self.rows_send.at[dz * 2 + dx], self.rows_arrive.at[j], to
+        )
+
+    def block_arrived(self, j):
+        part = self.block(j)
+        remote(
+            part, part, self.rows_send.at[0], self.rows_arrive.at[j], self.chain(0)
+        ).wait_recv()
+
+    def rows_onward(self, core):
+        zh, zl, y, x, c = self.at
+        j = x * 2 + core
+        part = self.block(j)
+        return remote(
+            part, part, self.rows_send.at[3 + core], self.rows_arrive.at[j], (zh, zl, y, 1 - x, c)
+        )
+
+    def near_rows(self):
+        zh, zl, y, x, c = self.at
+        j = x * 2 + c
+        self.rows_copy(0, 1).start()
+
+        @pl.when(c == zh)
+        def _():
+            pltpu.make_async_copy(self.rows, self.block(j), self.rows_arrive.at[j]).start()
+
+        @pl.when(c != zh)
+        def _():
+            self.rows_copy(0, 0).start()
+
+    def relay_rows(self):
+        zh, zl, y, x, c = self.at
+
+        @pl.when(c != zh)
+        def _():
+            for core in range(2):
+                self.block_arrived(x * 2 + core)
+                self.rows_onward(core).start()
+
+    def all_rows(self):
+        zh, zl, y, x, c = self.at
+        for j in range(4):
+            pl.when(jnp.logical_or(c == zh, x != j // 2))(lambda: self.block_arrived(j))
+
+    def drain_rows(self):
+        zh, zl, y, x, c = self.at
+        self.rows_copy(0, 1).wait_send()
+        self.rows_copy(1, 0).wait_send()
+
+        @pl.when(c != zh)
+        def _():
+            self.rows_copy(0, 0).wait_send()
+            self.rows_onward(0).wait_send()
+            self.rows_onward(1).wait_send()
+
+
+    def project(self, k, weights):
+        wide = weights.shape[2] // 2
         for part in range(2):
             columns = pl.ds(part * wide, wide)
-            product_ref[k, :, columns] = jnp.dot(
-                normed[...], full[k, :, columns], preferred_element_type=jnp.float32
-            ).astype(product_ref.dtype)
-
-    def write_out(k):
-        pltpu.make_async_copy(full.at[k], out_ref.at[k - UNITS_IN], out_sem.at[k - UNITS_IN]).start()
+            self.products[k, :, columns] = jnp.dot(
+                self.normed[...], weights[k, :, columns], preferred_element_type=jnp.float32
+            ).astype(self.products.dtype)
+
+    def rotate(self, unit, target, scale):
+        wide = KEY // 2
+
+        def rows(first):
+            lines = pl.ds(first, 128)
+            cosine, sine = self.cosine[lines], self.sine[lines]
+            for head in range(self.heads):
+                low = pl.ds(head * KEY, wide)
+                high = pl.ds(head * KEY + wide, wide)
+                front = self.products[unit, lines, low].astype(jnp.float32)
+                back = self.products[unit, lines, high].astype(jnp.float32)
+                target[lines, low] = ((front * cosine - back * sine) * scale).astype(target.dtype)
+                target[lines, high] = ((front * sine + back * cosine) * scale).astype(target.dtype)
+
+        self.by_rows(128, rows)
+
+    def contribute(self, head):
+        columns = pl.ds(head * KEY, KEY)
+        left = self.count - 1.0 - self.position(0, self.count)
+        trailing = jnp.exp(self.log_decay(head) * left)
+        weighted = (self.keys[:, columns].astype(jnp.float32) * trailing).astype(jnp.bfloat16)
+        total = lax.dot_general(
+            weighted,
+            self.products[1 + head],
+            (((0,), (0,)), ((), ())),
+            preferred_element_type=jnp.float32,
+        )
+        self.sending[pl.ds(head * KEY, KEY)] = total.astype(self.sending.dtype)
+
+    def slice_copy(self, s):
+        size = self.got.shape[1]
+        part = self.sending.at[pl.ds(s * size, size)]
+        return remote(
+            part,
+            self.got.at[self.link],
+            self.slice_sems.at[0, s],
+            self.slice_sems.at[1, self.link],
+            self.chain(s),
+        )
+
+    def prefix_copy(self, s):
+        size = self.got.shape[1]
+        lines = pl.ds(pl.multiple_of(self.link * size, size), size)
+        return remote(
+            self.prefix.at[s],
+            self.state.at[lines],
+            self.prefix_sems.at[0, s],
+            self.prefix_sems.at[1, self.link],
+            self.chain(s),
+        )
+
+    def others(self, what):
+        for s in range(self.links):
+            pl.when(self.link != s)(lambda: what(s))
+
+    def send_slices(self):
+        self.others(lambda s: self.slice_copy(s).start())
+        size = self.got.shape[1]
+        lines = pl.ds(pl.multiple_of(self.link * size, size), size)
+        self.got[self.link] = self.sending[lines]
+
+    def scan(self):
+        size = self.got.shape[1]
+
+        def arrived(s):
+            part = self.got.at[s]
+            remote(
+                part, part, self.slice_sems.at[0, s], self.slice_sems.at[1, s], self.chain(s)
+            ).wait_recv()
+
+        self.others(arrived)
+        step = jnp.exp(
+            jnp.full((1, 1), self.log_decay(self.link * size // KEY) * self.count, jnp.float32)
+        )
+        state = jnp.zeros(self.got.shape[1:], jnp.float32)
+        for s in range(self.links):
+            self.prefix[s] = state.astype(self.prefix.dtype)
+            state = state * step + self.got[s].astype(jnp.float32)
+        self.others(lambda s: self.prefix_copy(s).start())
+        lines = pl.ds(pl.multiple_of(self.link * size, size), size)
+        self.state[lines] = self.prefix[self.link]
+
+    def state_arrived(self):
+        size = self.got.shape[1]
+
+        def arrived(s):
+            part = self.state.at[pl.ds(s * size, size)]
+            remote(
+                part, part, self.prefix_sems.at[0, s], self.prefix_sems.at[1, s], self.chain(s)
+            ).wait_recv()
+
+        self.others(arrived)
+
+    def inside(self, head):
+        columns = pl.ds(head * KEY, KEY)
+        decay = self.log_decay(head)
+
+        def rows(first):
+            lines = pl.ds(first, 128)
+            scores = contract(self.queries[lines, columns], self.keys[:, columns])
+            later = lax.broadcasted_iota(jnp.int32, scores.shape, 0) + first
+            ahead = later - lax.broadcasted_iota(jnp.int32, scores.shape, 1)
+            weight = jnp.exp(decay * jnp.maximum(ahead, 0).astype(jnp.float32))
+            scores = jnp.where(ahead >= 0, scores * weight, 0.0).astype(jnp.bfloat16)
+            self.within[head, lines] = jnp.dot(
+                scores, self.products[1 + head], preferred_element_type=jnp.float32
+            )
+
+        self.by_rows(128, rows)
+
+    def finish_head(self, head):
+        columns = pl.ds(head * KEY, KEY)
+        decay = self.log_decay(head)
+
+        def rows(first):
+            lines = pl.ds(first, 128)
+            cross = jnp.dot(
+                self.queries[lines, columns],
+                self.state[pl.ds(head * KEY, KEY)],
+                preferred_element_type=jnp.float32,
+            )
+            leading = jnp.exp(decay * (self.position(first, 128) + 1.0))
+            raw = self.within[head, lines] + cross * leading
+            average = jnp.mean(raw, axis=-1, keepdims=True)
+            centred = raw - average
+            wide = jnp.mean(jnp.square(centred), axis=-1, keepdims=True)
+            switch = self.products[7 + head, lines].astype(jnp.float32)
+            result = centred * lax.rsqrt(wide + group_eps) * jax.nn.silu(switch)
+            self.hidden[lines, pl.ds(head * VAL, VAL)] = result.astype(self.hidden.dtype)
+
+        self.by_rows(128, rows)
+
+
+    def glu(self):
+        lead = self.halo_in.shape[0]
+
+        def rows(first):
+            lines = pl.ds(first, 128)
+            value = self.products[4, lines].astype(jnp.float32)
+            switch = self.products[5, lines].astype(jnp.float32)
+            gated = (value * jax.nn.sigmoid(switch)).astype(jnp.bfloat16)
+            self.padded[pl.ds(pl.multiple_of(first + lead, 8), 128)] = gated.astype(jnp.float32)
+
+        self.by_rows(128, rows)
+        self.halo_out[...] = self.padded[pl.ds(self.count, lead)].astype(jnp.bfloat16)
+        self.padded[pl.ds(self.count + lead, 8)] = jnp.zeros(
+            (8, self.padded.shape[1]), jnp.float32
+        )
+        pl.when(self.link < self.links - 1)(lambda: self.halo_copy().start())
+
+    def halo_copy(self):
+        following = jnp.minimum(self.link + 1, self.links - 1)
+        return remote(
+            self.halo_out,
+            self.halo_in,
+            self.halo_sems.at[0],
+            self.halo_sems.at[1],
+            self.chain(following),
+        )
+
+    def convolve(self):
+        lead = self.halo_in.shape[0]
+        channels = self.padded.shape[1]
+
+        @pl.when(self.link > 0)
+        def _():
+            self.halo_copy().wait_recv()
+            self.padded[pl.ds(0, lead)] = self.halo_in[...].astype(jnp.float32)
+
+        @pl.when(self.link == 0)
+        def _():
+            self.padded[pl.ds(0, lead)] = jnp.zeros((lead, channels), jnp.float32)
+
+        size = 64
+        lanes = 128
+
+        def body(n, carry):
+            first = pl.multiple_of(n * size, size)
+            for part in range(channels // lanes):
+                columns = pl.ds(part * lanes, lanes)
+                spot = pl.multiple_of(self.rank * channels + part * lanes, lanes)
+                weights = self.taps[:, pl.ds(spot, lanes)]
+                source = self.padded[pl.ds(first, size + lead + 8), columns]
+                total = None
+                for low in range(8):
+                    group = None
+                    for high in range(lead // 8 + 1):
+                        tap = high * 8 + low - (lead - KW + 1)
+                        if not 0 <= tap < KW:
+                            continue
+                        term = source[high * 8 : high * 8 + size + 8] * weights[tap : tap + 1]
+                        group = term if group is None else group + term
+                    if low:
+                        group = pltpu.roll(group, size + 8 - low, 0)
+                    total = group[:size] if total is None else total + group[:size]
+                self.summed[pl.ds(first, size), columns] = total
+            return carry
+
+        lax.fori_loop(0, self.count // size, body, 0)
+
+    def finish_convolution(self):
+        channels = self.padded.shape[1]
+        spot = pl.ds(pl.multiple_of(self.rank * channels, channels), channels)
+        gain, shift = self.gain[:, spot], self.shift[:, spot]
+
+        def rows(first):
+            lines = pl.ds(first, 128)
+            total = self.summed[lines]
+            average = jnp.mean(total, axis=-1, keepdims=True)
+            centred = total - average
+            wide = jnp.mean(jnp.square(centred), axis=-1, keepdims=True)
+            normalized = centred * lax.rsqrt(wide + layer_eps) * gain + shift
+            switch = self.products[6, lines].astype(jnp.float32)
+            result = jax.nn.silu(normalized) * jax.nn.silu(switch)
+            target = pl.ds(self.heads * VAL, channels)
+            self.hidden[lines, target] = result.astype(self.hidden.dtype)
+
+        self.by_rows(128, rows)
+
+
+    def x_copy(self, n):
+        zh, zl, y, x, c = self.at
+        return remote(
+            self.sent.at[n],
+            self.crossed.at[n],
+            self.out_sems.at[0, n],
+            self.out_sems.at[1, n],
+            (zh, zl, y, 1 - x, c),
+        )
+
+    def near_copy(self, n):
+        zh, zl, y, x, c = self.at
+        share = self.out.shape[0]
+        part = self.half.at[n, pl.ds(pl.multiple_of((1 - c) * share, share), share)]
+        return remote(
+            part,
+            self.here.at[n],
+            self.out_sems.at[2, n],
+            self.out_sems.at[3, n],
+            (zh, zl, y, x, 1 - c),
+        )
+
+    def far_copy(self, n, core):
+        zh, zl, y, x, c = self.at
+        share = self.out.shape[0]
+        return remote(
+            self.half.at[n, pl.ds(core * share, share)],
+            self.there.at[n],
+            self.out_sems.at[2 + 2 * core, n],
+            self.out_sems.at[5, n],
+            (c, zl, y, x, core),
+        )
+
+    def multiply(self, j, q, weights):
+        x = self.at[3]
+        tile = self.sent.shape[2]
+        n = j * 4 + q
+        pair = self.sent.shape[1]
+        total = contract(self.hidden[...], weights[j, pl.ds(q * tile, tile)])
+        low, high = total[:pair], total[pair:]
+        self.kept[n] = jnp.where(x == 0, low, high)
+        self.sent[n] = jnp.where(x == 0, high, low).astype(self.sent.dtype)
+        self.x_copy(n).start()
+
+    def join(self, n):
+        zh, zl, y, x, c = self.at
+        self.x_copy(n).wait_recv()
+        total = self.kept[n] + self.crossed[n].astype(jnp.float32)
+        self.half[n] = total.astype(self.half.dtype)
+
+        @pl.when(c == zh)
+        def _():
+            self.near_copy(n).start()
+
+        @pl.when(c != zh)
+        def _():
+            self.far_copy(n, 0).start()
+            self.far_copy(n, 1).start()
+
+    def close(self, j, q):
+        zh, zl, y, x, c = self.at
+        n = j * 4 + q
+        share = self.out.shape[0]
+        wide = self.sent.shape[2] // 2
+        part = self.there.at[n]
+        remote(
+            part, part, self.out_sems.at[4, n], self.out_sems.at[5, n], (zh, zl, y, 1 - x, c)
+        ).wait_recv()
+        far_part = self.there[n].astype(jnp.float32)
+
+        def store(near_part):
+            total = (near_part.astype(jnp.float32) + far_part).astype(self.out.dtype)
+            for k in range(2):
+                spot = ((2 * q + k) * 2 + j) * wide
+                self.out[:, pl.ds(spot, wide)] = total[:, k * wide : (k + 1) * wide]
+
+        @pl.when(c == zh)
+        def _():
+            store(self.half[n, pl.ds(pl.multiple_of(c * share, share), share)])
+
+        @pl.when(c != zh)
+        def _():
+            self.near_copy(n).wait_recv()
+            store(self.here[n])
+
+    def drain(self):
+        zh, zl, y, x, c = self.at
+        self.drain_rows()
+        self.others(lambda s: self.slice_copy(s).wait_send())
+        self.others(lambda s: self.prefix_copy(s).wait_send())
+        pl.when(self.link < self.links - 1)(lambda: self.halo_copy().wait_send())
+        for n in range(self.sent.shape[0]):
+            self.x_copy(n).wait_send()
+
+            @pl.when(c == zh)
+            def _():
+                self.near_copy(n).wait_send()
+
+            @pl.when(c != zh)
+            def _():
+                self.far_copy(n, 0).wait_send()
+                self.far_copy(n, 1).wait_send()
+
+
+def layer_kernel(layout, out_layout, *refs):
+    blocks, refs = refs[:9], refs[9:]
+    first_gather, refs = refs[-12:-6], refs[:-12] + refs[-6:]
+    second_gather, refs = refs[-6:], refs[:-6]
+    layer = Layer(refs)
+    inward, outward = Gather(*first_gather), Gather(*second_gather)
+    units = len(layout)
+    total = units + 2
+
+    layer.near_rows()
+    for k, (which, first) in enumerate(layout):
+        inward.load(k, blocks[which].at[:, pl.ds(first, inward.source.shape[2])], None)
+    for k, parts in enumerate(out_layout):
+        for which, row, column in parts:
+            ref = blocks[which]
+            lines = pl.ds(row, outward.depth)
+            outward.load(k, ref.at[lines], pl.ds(column, ref.shape[1]))
+
+    for k in range(AHEAD):
+        inward.begin(k)
+        if k == ROWS_AFTER:
+            layer.rows_copy(1, 0).start()
+
+    def at_unit(k, what):
+        @pl.when(jnp.logical_and(k >= 0, k < units))
+        def _():
+            what(inward, k)
+
+        @pl.when(jnp.logical_and(k >= units, k < total))
+        def _():
+            what(outward, k - units)
+
+    after = (
+        (lambda: layer.rotate(0, layer.keys, KEY ** (-0.5)),),
+        (lambda: layer.contribute(0),),
+        (lambda: layer.contribute(1), layer.send_slices),
+        (lambda: layer.rotate(3, layer.queries, 1.0), layer.scan),
+        (lambda: layer.inside(0),),
+        (layer.glu, lambda: layer.inside(1)),
+        (layer.convolve,),
+        (layer.finish_convolution, layer.state_arrived, lambda: layer.finish_head(0)),
+        (lambda: layer.finish_head(1),),
+    )
 
     def step(i, carry):
-        when_unit(i, units, lambda k: gather.stage(k, 0))
-        when_unit(i - 1, units, lambda k: gather.stage(k, 1))
-        when_unit(i - 2, units, lambda k: gather.stage(k, 2))
-        when_unit(i + AHEAD, units, gather.begin)
-        when_unit(i - 3, units, gather.complete)
-        when_unit(i - 3, UNITS_IN, project)
-
-        @pl.when(i - 3 >= UNITS_IN)
-        def _():
-            write_out(i - 3)
+        for number in range(3):
+            at_unit(i - LAGS[number], lambda gather, k: gather.stage(k, number))
+        at_unit(i + AHEAD, lambda gather, k: gather.begin(k))
+        pl.when(i == ROWS_RELAY)(layer.relay_rows)
+        done = i - LAGS[3]
+        pl.when(done == 0)(layer.all_rows)
+
+        @pl.when(jnp.logical_and(done >= 0, done < units))
+        def _():
+            inward.complete(done)
+            layer.project(done, inward.full)
+
+        for k, events in enumerate(after):
+
+            @pl.when(done == k)
+            def _():
+                for event in events:
+                    event()
 
         return carry
 
-    lax.fori_loop(0, units + 3, step, 0)
-
-    def finish(k, carry):
-        gather.drain(k)
-        return carry
-
-    lax.fori_loop(0, units, finish, 0)
-    for dz, dx in far_rows:
-        rows_copy(dz, dx).wait_send()
-
-    @pl.when(c != zh)
-    def _():
-        rows_copy(0, 0).wait_send()
-
-    for k in range(units - UNITS_IN):
-        pltpu.make_async_copy(full.at[UNITS_IN + k], out_ref.at[k], out_sem.at[k]).wait()
-
-
-def gather_and_project(rows, blocks, width):
-    layout = [(n, first) for n, b in enumerate(blocks) for first in range(0, b.shape[1], width)]
+    lax.fori_loop(0, units + LAGS[3], step, 0)
+
+    def output(j):
+        outward.complete(j)
+        for q in range(4):
+            layer.multiply(j, q, outward.full)
+
+    def late_stages(j):
+        for number in range(3):
+            if units + j + LAGS[number] >= units + LAGS[3]:
+                outward.stage(j, number)
+
+    late_stages(0)
+    output(0)
+    late_stages(1)
+    for n in range(4):
+        layer.join(n)
+    output(1)
+    for q in range(4):
+        layer.close(0, q)
+    for n in range(4, 8):
+        layer.join(n)
+    for q in range(4):
+        layer.close(1, q)
+
+    def finish(gather):
+        def body(k, carry):
+            gather.drain(k)
+            return carry
+
+        lax.fori_loop(0, gather.source.shape[0], body, 0)
+
+    finish(inward)
+    finish(outward)
+    layer.drain()
+
+
+def whole_layer(rows, cosine, sine, taps, gain, shift, blocks):
+    depth, width = blocks[0].shape
+    share, model = rows.shape
+    layout = []
+    for which, block in enumerate(blocks[:7]):
+        layout += [(which, first) for first in range(0, block.shape[1], width)]
     units = len(layout)
-    depth, shares, dtype = blocks[0].shape[0], 8, rows.dtype
-    span = 4 * rows.shape[0]
+    shares, dtype = 8, rows.dtype
+    span = 4 * share
+    inner_width = blocks[7].shape[1] + blocks[8].shape[1]
+    half_depth = depth // 2
+    out_layout = [
+        ((7, j * half_depth, 0), (8, j * half_depth, blocks[7].shape[1])) for j in range(2)
+    ]
+    heads = width // KEY
+    channels = blocks[8].shape[1]
+    lead = (KW + 7) // 8 * 8
+    tile = 2 * half_depth
+    tiles = model // tile
+    sem = pltpu.SemaphoreType.DMA
+    slice_rows = heads * KEY // shares
     return pl.pallas_call(
-        lambda *refs: gather_kernel(layout, units, *refs),
-        out_shape=[
-            jax.ShapeDtypeStruct((UNITS_IN, span, width), dtype),
-            jax.ShapeDtypeStruct((units - UNITS_IN, shares * depth, width), dtype),
-        ],
-        in_specs=[pl.BlockSpec(memory_space=pl.ANY)] * (1 + len(blocks)),
-        out_specs=[pl.BlockSpec(memory_space=pltpu.VMEM), pl.BlockSpec(memory_space=pl.ANY)],
-        scratch_shapes=[pltpu.VMEM((span, rows.shape[1]), dtype)]
-        + gather_scratch(units, depth, width, shares, dtype)
-        + [
-            pltpu.SemaphoreType.DMA((4,)),
-            pltpu.SemaphoreType.DMA((4,)),
-            pltpu.SemaphoreType.DMA((units - UNITS_IN,)),
-        ],
-        compiler_params=pltpu.CompilerParams(has_side_effects=True, vmem_limit_bytes=56 << 20),
-        name="gather_project",
-    )(rows, *blocks)
-
-
-def finish_kernel(tile, first, second, third, matrix, out, kept, sent, got, half, here, there, sems):
-    hidden = (first, second, third)
-    zh, zl, y, x, c = place()
-    tiles = matrix.shape[1] // tile
-    share = out.shape[0]
-    pair = 2 * share
-    to_x, from_x, to_near, from_near, to_far, from_far = (sems.at[k] for k in range(6))
-    across, sibling = (zh, zl, y, 1 - x, c), (zh, zl, y, x, 1 - c)
-    stays = c == zh
-
-    def x_copy(n):
-        return remote(sent.at[n], got.at[n], to_x.at[n], from_x.at[n], across)
-
-    def near_copy(n):
-        part = half.at[n, pl.ds(pl.multiple_of((1 - c) * share, share), share)]
-        return remote(part, here.at[n], to_near.at[n], from_near.at[n], sibling)
-
-    def far_copy(n, core):
-        part = half.at[n, pl.ds(core * share, share)]
-        out_sem = (to_near if core == 0 else to_far).at[n]
-        return remote(part, there.at[n], out_sem, from_far.at[n], (c, zl, y, x, core))
-
-    def multiply(n):
-        lines = pl.ds(pl.multiple_of(n * tile, tile), tile)
-        total = contract(hidden[0][...], matrix[0, lines])
-        total += contract(hidden[1][...], matrix[1, lines])
-        total += contract(hidden[2][...], matrix[2, lines])
-        low, high = total[:pair], total[pair:]
-        kept[n] = jnp.where(x == 0, low, high)
-        sent[n] = jnp.where(x == 0, high, low).astype(sent.dtype)
-        x_copy(n).start()
-
-    def join(n):
-        x_copy(n).wait_recv()
-        half[n] = (kept[n] + got[n].astype(jnp.float32)).astype(half.dtype)
-
-        @pl.when(stays)
-        def _():
-            near_copy(n).start()
-
-        @pl.when(jnp.logical_not(stays))
-        def _():
-            far_copy(n, 0).start()
-            far_copy(n, 1).start()
-
-    def close(n):
-        remote(there.at[n], there.at[n], to_far.at[n], from_far.at[n], across).wait_recv()
-        lines = pl.ds(pl.multiple_of(n * tile, tile), tile)
-        far_part = there[n].astype(jnp.float32)
-
-        @pl.when(stays)
-        def _():
-            mine = half[n, pl.ds(pl.multiple_of(c * share, share), share)].astype(jnp.float32)
-            out[:, lines] = (mine + far_part).astype(out.dtype)
-
-        @pl.when(jnp.logical_not(stays))
-        def _():
-            near_copy(n).wait_recv()
-            out[:, lines] = (here[n].astype(jnp.float32) + far_part).astype(out.dtype)
-
-    def when_tile(n, what):
-        @pl.when(jnp.logical_and(n >= 0, n < tiles))
-        def _():
-            what(n)
-
-    def step(i, carry):
-        when_tile(i, multiply)
-        when_tile(i - 3, join)
-        when_tile(i - 6, close)
-        return carry
-
-    lax.fori_loop(0, tiles + 6, step, 0)
-
-    def drain(n, carry):
-        x_copy(n).wait_send()
-
-        @pl.when(stays)
-        def _():
-            near_copy(n).wait_send()
-
-        @pl.when(jnp.logical_not(stays))
-        def _():
-            far_copy(n, 0).wait_send()
-            far_copy(n, 1).wait_send()
-
-        return carry
-
-    lax.fori_loop(0, tiles, drain, 0)
-
-
-def finish_outputs(hidden, matrix, tile):
-    span = hidden[0].shape[0]
-    share = span // 4
-    tiles = matrix.shape[1] // tile
-    dtype = matrix.dtype
-    return pl.pallas_call(
-        lambda *refs: finish_kernel(tile, *refs),
-        out_shape=jax.ShapeDtypeStruct((share, matrix.shape[1]), dtype),
-        in_specs=[pl.BlockSpec(memory_space=pltpu.VMEM)] * 4,
+        lambda *refs: layer_kernel(layout, out_layout, *refs),
+        out_shape=jax.ShapeDtypeStruct((share, model), dtype),
+        in_specs=[pl.BlockSpec(memory_space=pl.ANY)] * 10
+        + [pl.BlockSpec(memory_space=pltpu.VMEM)] * 5,
         out_specs=pl.BlockSpec(memory_space=pltpu.VMEM),
         scratch_shapes=[
+            pltpu.VMEM((span, model), dtype),
+            pltpu.VMEM((units, span, width), dtype),
+            pltpu.VMEM((span, width), dtype),
+            pltpu.VMEM((span, width), dtype),
+            pltpu.VMEM((heads, span, VAL), jnp.float32),
+            pltpu.VMEM((heads * KEY, VAL), dtype),
+            pltpu.VMEM((shares, slice_rows, VAL), dtype),
+            pltpu.VMEM((shares, slice_rows, VAL), dtype),
+            pltpu.VMEM((heads * KEY, VAL), dtype),
+            pltpu.VMEM((span + lead + 8, channels), jnp.float32),
+            pltpu.VMEM((lead, channels), dtype),
+            pltpu.VMEM((lead, channels), dtype),
+            pltpu.VMEM((span, channels), jnp.float32),
+            pltpu.VMEM((span, inner_width), dtype),
             pltpu.VMEM((tiles, 2 * share, tile), jnp.float32),
             pltpu.VMEM((tiles, 2 * share, tile), dtype),
             pltpu.VMEM((tiles, 2 * share, tile), dtype),
             pltpu.VMEM((tiles, 2 * share, tile), dtype),
             pltpu.VMEM((tiles, share, tile), dtype),
             pltpu.VMEM((tiles, share, tile), dtype),
-            pltpu.SemaphoreType.DMA((6, tiles)),
-        ],
-        compiler_params=pltpu.CompilerParams(has_side_effects=True, vmem_limit_bytes=56 << 20),
-        name="finish",
-    )(*hidden, matrix)
-
-
-def shifted(x, by):
-    length, cores = lax.axis_size(CHAIN), lax.axis_size("c")
-    inner = length // cores
-    spot = [(i % inner) * cores + i // inner for i in range(length)]
-    return lax.ppermute(x, ("zl", "y", "c"), list(zip(spot[:-by], spot[by:])))
+            sem((5,)),
+            sem((4,)),
+            sem((2, shares)),
+            sem((2, shares)),
+            sem((2,)),
+            sem((6, tiles)),
+        ]
+        + gather_scratch(units, depth, width, shares, dtype)
+        + gather_scratch(2, half_depth, inner_width, shares, dtype),
+        compiler_params=pltpu.CompilerParams(has_side_effects=True, vmem_limit_bytes=60 << 20),
+        name="layer",
+    )(*blocks, rows, cosine, sine, taps, gain, shift)
 
 
 def local_squares(
@@ -690,48 +1092,24 @@
     retain_output,
     convolve_output,
 ):
-    rank = lax.axis_index("x") * 2 + lax.axis_index("zh")
-    groups = 4
-    chain_length = lax.axis_size(CHAIN)
     chain_rank = lax.axis_index(CHAIN)
     normed = rms_normalize(tokens, norm_gain)
+    row_count = normed.shape[0] * 4
+    half_width = KEY // 2
+    frequency = rope_base ** (-jnp.arange(half_width, dtype=jnp.float32) / half_width)
+    positions = chain_rank * row_count + jnp.arange(row_count, dtype=jnp.int32)
+    angles = positions.astype(jnp.float32)[:, None] * frequency
     blocks = (key_weight, value_weight, query_weight, unit_value, unit_gate, convolve_gate)
     blocks += (retain_gate, retain_output, convolve_output)
-    products, matrix = gather_and_project(normed, blocks, key_weight.shape[1])
-    keys, value_0, value_1, queries, glu_value, glu_switch, convolve_switch, gate_0, gate_1 = (
-        products[k] for k in range(UNITS_IN)
+    return whole_layer(
+        normed,
+        jnp.cos(angles),
+        jnp.sin(angles),
+        filter_taps,
+        layer_gain[None],
+        layer_shift[None],
+        blocks,
     )
-    row_count = keys.shape[0]
-    local_heads = 2
-    positions = chain_rank * row_count + jnp.arange(row_count, dtype=jnp.int32)
-    log_decay = decay_logs(
-        rank * local_heads, local_heads, local_heads * groups, row_count * chain_length
-    )
-    values = jnp.concatenate([value_0, value_1], axis=1)
-    rotated_query, rotated_keys, value_heads = prepare(queries, keys, values, positions)
-    within, contribution = local_parts(rotated_query, rotated_keys, value_heads, log_decay)
-    gated_input = (
-        glu_value.astype(jnp.float32) * jax.nn.sigmoid(glu_switch.astype(jnp.float32))
-    ).astype(jnp.bfloat16)
-    channels = gated_input.shape[1]
-    before = shifted(gated_input[row_count - (KW - 1) :], 1)
-    log_span = log_decay * row_count
-    state = shifted(contribution.astype(jnp.bfloat16), 1).astype(jnp.float32)
-    by = 1
-    while by < chain_length:
-        earlier = shifted(state.astype(jnp.bfloat16), by).astype(jnp.float32)
-        state = state + jnp.exp(log_span * by)[:, None, None] * earlier
-        by *= 2
-    raw = within + cross_part(rotated_query, state, log_decay)
-    retain_hidden = retain_finish(raw, jnp.concatenate([gate_0, gate_1], axis=1))
-    tap_slice = lax.dynamic_slice_in_dim(filter_taps, rank * channels, channels, 1)
-    gain_slice = lax.dynamic_slice_in_dim(layer_gain, rank * channels, channels, 0)
-    shift_slice = lax.dynamic_slice_in_dim(layer_shift, rank * channels, channels, 0)
-    convolve_hidden = convolve_branch(
-        gated_input, before, tap_slice, gain_slice, shift_slice, convolve_switch
-    )
-    hidden = (retain_hidden[:, :VAL], retain_hidden[:, VAL:], convolve_hidden)
-    return finish_outputs(hidden, matrix, 256)
 
 
 def squares(mesh):

time: 316 us -> 204 us (0.65); the launches traced: 312 us -> 204 us
  other arithmetic: 40.4 us -> 4.13 us
  Pallas kernels: 222 us -> 198 us
  waiting for transfers between devices: 21.3 us -> 0 us
  local copies, waits for them, and re-layouts: 13.1 us -> 1.89 us
  starting transfers between devices: 9.69 us -> 0 us
  matrix products: 4.88 us -> 0 us
    pallas_call x2 -> x1, Pallas kernels: 222 us -> 198 us  [whole_layer(): pl.pallas_call(lambda *refs: layer_kernel(layout, out_layout, *refs), out...]
    ppermute x5 -> x0, waiting for transfers between devices: 21.3 us -> none  [shifted(): return lax.ppermute(x, ('zl', 'y', 'c'), list(zip(spot[:-by], spot[by:])))]
    reduce_sum x3 -> x0, other arithmetic: 18.2 us -> none  [the longest x1 17.6 us: convolve_branch(): average = jnp.mean(grouped, axis=-1, keepdims=True)]
    ppermute x5 -> x0, starting transfers between devices: 9.69 us -> none  [shifted(): return lax.ppermute(x, ('zl', 'y', 'c'), list(zip(spot[:-by], spot[by:])))]
    convert_element_type x7 -> x1, other arithmetic: 8.13 us -> 0.01 us  [local_squares(): angles = positions.astype(jnp.float32)[:, None] * frequency]
    slice x5 -> x0, local copies, waits for them, and re-layouts: 4.88 us -> none  [the longest x2 3.09 us: convolve_branch(): tap_slice[tap_index]]
    dot_general x3 -> x0, matrix products: 4.88 us -> none  [the longest x1 3.3 us: local_parts(): jnp.einsum('hij,jhe->ihe', scores, values, preferred_element_type=jnp.flo...]
    squeeze x1 -> x0, other arithmetic: 3.42 us -> none  [local_squares(): products[k]]
  transfers between devices with their start and end apart: 5 -> 0, of which waited for: 3 -> 0; matrix products, arithmetic and copies ran while one was open for 14% -> 0% of each run, Pallas kernels for 0% -> 0%
where the time goes in v2:
time: 204 us
  Pallas kernels  198 us (97%)
  other arithmetic  4.13 us (2%)
    pallas_call x1, Pallas kernels, whole_layer(): pl.pallas_call(lambda *refs: layer_kernel(layout, out_layout, *refs), out...  198 us

profile of v2, /device:TPU:9, one launch (start us, length us, event | category | flops | bytes accessed | tf_op | source)
XLA Modules:
  0.0 203.7 jit_solution(8394854622858848461)
XLA Ops:
  0.0 0.0 copy-start
  0.0 1.3 fusion
  1.3 0.0 copy-start.1
  1.3 1.8 multiply_sine_fusion
  3.2 0.0 copy-done
  3.2 0.0 copy-done.1
  3.2 1.0 fusion.2.refs_9_
  4.2 197.6 %layer.1 = bf16[128,2048]{1,0:T(8,128)(2,1)} custom-call(bf16[256,512]{1,0:T(8,128)(2,1)} %refs_0_.1, bf16[256,1024]{1,0:T(8,128)(2,1)} %refs_1_.1, bf16[256,512]{1,0:T(8,128)(2,1)} %refs_2_.1, bf16[256,512]{1,0:T(8,128)(2,1)} %refs_3_.1, bf16[256,512]{1,0:T(8,128)(2,1)} %refs_4_.1, bf16[256,512]{1,0:T(8,128)(2,1)} %refs_5_.1, bf16[256,1024]{1,0:T(8,128)(2,1)} %refs_6_.1, ...), custom_call_target="tpu_custom_call" | custom-call | tf_op jit(solution)/shard_map/layer/pallas_call | solution.py:1038
  201.8 1.9 copy.16
  (3 shorter events, 0.0 us)
Async XLA Ops:
  0.0 3.2 %copy-start = (bf16[128,2048]{1,0:T(8,128)(2,1)S(1)}, bf16[128,2048]{1,0:T(8,128)(2,1)}, u32[]{:S(2)}) copy-start(bf16[128,2048]{1,0:T(8,128)(2,1)} %param.14) | copy-start | bytes 1572868
  1.3 1.8 copy-start.1

commit v3 on v2

--- a/solution.py
+++ b/solution.py
@@ -2,6 +2,7 @@
 
 import jax
 import jax.numpy as jnp
+import numpy as np
 from jax import lax
 from jax.experimental import pallas as pl
 from jax.experimental.pallas import tpu as pltpu
@@ -209,10 +210,13 @@
     return swap_planes(lax.psum_scatter(mixed, "hi", scatter_dimension=0, tiled=True))
 
 
-AHEAD = 5
-LAGS = (0, 2, 3, 4)
-ROWS_AFTER = 2
-ROWS_RELAY = 3
+OWN_AHEAD = 4
+FAR_AHEAD = 2
+LEADS = (1, 1, 0, -1, 0)
+STRIPS = 4
+ROWS_RELAY = 1
+START = 4
+BEHIND = 1
 MESH = pl.DeviceIdType.MESH
 SQUARE = ("zh", "zl", "y", "x", "c")
 CHAIN = ("c", "zl", "y")
@@ -313,18 +317,10 @@
             )
         return copies
 
-    def begin(self, k):
+    def begin(self, k, own):
         pltpu.make_async_copy(self.source.at[k], self.source.at[k], self.near.at[k]).wait()
-
-        @pl.when(self.is_own)
-        def _():
-            for copy in self.own_sends(k):
-                copy.start()
-
-        @pl.when(jnp.logical_not(self.is_own))
-        def _():
-            for copy in self.far_sends(k):
-                copy.start()
+        for copy in self.own_sends(k) if own else self.far_sends(k):
+            copy.start()
 
     def onward(self, k, s, device, slot):
         piece = self.rows(k, s, self.at[4])
@@ -343,17 +339,20 @@
             (
                 (self.far(0, 0), ((z_mate, 0, None), (y_mate, 1, None), (sibling, 2, None))),
                 (self.far(1, 0), ((z_mate, 3, None), (y_mate, 4, None), (sibling, 5, None))),
+            ),
+            (
                 (self.own(0, 1), ((z_mate, 8, 0), (sibling, 7, None))),
                 (self.own(1, 0), ((sibling, 6, None),)),
             ),
             (
                 (self.far(0, 1), ((sibling, 9, None),)),
                 (self.far(1, 1), ((sibling, 10, None),)),
-                (self.own(1, 1), ((sibling, 11, None),)),
             ),
             (),
+            ((self.own(1, 1), ((sibling, 11, None),)),),
         )
         outer = (
+            (),
             (
                 (self.own(1, 1), ((z_mate, 2, None), (sibling, 3, None))),
                 (self.own(0, 0), ((y_mate, 1, 1), (sibling, 0, None))),
@@ -363,10 +362,10 @@
                 (self.far(1, 0), ((y_mate, 6, None), (sibling, 7, None))),
             ),
             (
-                (self.own(0, 1), ((sibling, 10, None),)),
                 (self.far(0, 1), ((sibling, 8, None),)),
                 (self.far(1, 1), ((sibling, 9, None),)),
             ),
+            ((self.own(0, 1), ((sibling, 10, None),)),),
         )
         return inner, outer
 
@@ -386,18 +385,10 @@
                         else:
                             pl.when(self.at[4] == lane)(copy.start)
 
-    def complete(self, k):
+    def complete_own(self, k):
         other = 1 - self.at[4]
-        for s in (
-            self.own(1 - self.outer, 0),
-            self.own(self.outer, 1),
-            self.own(1 - self.outer, 1),
-            self.far(0, 0),
-            self.far(1, 0),
-            self.far(0, 1),
-            self.far(1, 1),
-        ):
-            self.landed(k, s, other)
+        for outer, flip in ((1 - self.outer, 0), (self.outer, 1), (1 - self.outer, 1)):
+            self.landed(k, self.own(outer, flip), other)
 
         @pl.when(jnp.logical_not(self.is_own))
         def _():
@@ -406,6 +397,11 @@
                 part, part, self.send.at[k, 0], self.beside.at[k], self.sibling()
             ).wait_recv()
 
+    def complete_far(self, k):
+        other = 1 - self.at[4]
+        for outer, flip in ((0, 0), (1, 0), (0, 1), (1, 1)):
+            self.landed(k, self.far(outer, flip), other)
+
     def drain(self, k):
         @pl.when(self.is_own)
         def _():
@@ -421,7 +417,7 @@
 
             @pl.when(self.outer == role)
             def _():
-                for number in range(3):
+                for number in range(len(moves)):
                     for s, targets in moves[number]:
                         for device, slot, lane in targets:
                             copy = self.onward(k, s, device, slot)
@@ -445,13 +441,20 @@
 class Layer:
     def __init__(self, refs):
         names = (
+            "tokens_in",
+            "angles_in",
+            "turns",
+            "taps_in",
+            "norm_gain",
+            "gain",
+            "shift",
+            "out",
+            "tokens",
+            "angles",
+            "taps",
             "rows",
             "cosine",
             "sine",
-            "taps",
-            "gain",
-            "shift",
-            "out",
             "normed",
             "products",
             "keys",
@@ -483,6 +486,7 @@
             self.prefix_sems,
             self.halo_sems,
             self.out_sems,
+            self.load_sems,
         ) = sems
         zh, zl, y, x, c = self.at = place()
         self.count = self.normed.shape[0]
@@ -502,12 +506,14 @@
         )
         return (math.log(0.05) + ratio * math.log(18.0)) / (self.count * self.links)
 
-    def by_rows(self, size, what):
+    def by_rows(self, what, slot=0, slots=1, size=128):
+        steps = self.count // size // slots
+
         def body(n, carry):
             what(pl.multiple_of(n * size, size))
             return carry
 
-        lax.fori_loop(0, self.count // size, body, 0)
+        lax.fori_loop(slot * steps, (slot + 1) * steps, body, 0)
 
     def position(self, first, size):
         rows = lax.broadcasted_iota(jnp.int32, (size, 1), 0) + first
@@ -518,76 +524,125 @@
         share = self.rows.shape[0]
         return self.normed.at[pl.ds(pl.multiple_of(j * share, share), share)]
 
-    def rows_copy(self, dz, dx):
+    def strip(self, j, t):
+        share = self.rows.shape[0]
+        size = share // STRIPS
+        return self.normed.at[pl.ds(pl.multiple_of(j * share + t * size, size), size)]
+
+    def near_copy_of_rows(self, dx):
         zh, zl, y, x, c = self.at
         j = x * 2 + c
-        to = (1 - zh if dz else zh, zl, y, 1 - x if dx else x, zh)
         return remote(
-            self.rows, self.block(j), self.rows_send.at[dz * 2 + dx], self.rows_arrive.at[j], to
-        )
-
-    def block_arrived(self, j):
-        part = self.block(j)
-        remote(
-            part, part, self.rows_send.at[0], self.rows_arrive.at[j], self.chain(0)
-        ).wait_recv()
-
-    def rows_onward(self, core):
+            self.rows,
+            self.block(j),
+            self.rows_send.at[dx],
+            self.rows_arrive.at[j, 0],
+            (zh, zl, y, 1 - x if dx else x, zh),
+        )
+
+    def far_strip(self, t):
+        zh, zl, y, x, c = self.at
+        j = x * 2 + c
+        size = self.rows.shape[0] // STRIPS
+        return remote(
+            self.rows.at[pl.ds(pl.multiple_of(t * size, size), size)],
+            self.strip(j, t),
+            self.rows_send.at[2 + t],
+            self.rows_arrive.at[j, t],
+            (1 - zh, zl, y, x, zh),
+        )
+
+    def onward_strip(self, core, t):
         zh, zl, y, x, c = self.at
         j = x * 2 + core
-        part = self.block(j)
         return remote(
-            part, part, self.rows_send.at[3 + core], self.rows_arrive.at[j], (zh, zl, y, 1 - x, c)
-        )
+            self.strip(j, t),
+            self.strip(j, t),
+            self.rows_send.at[2 + (1 + core) * STRIPS + t],
+            self.rows_arrive.at[j, t],
+            (zh, zl, y, 1 - x, c),
+        )
+
+    def rows_landed(self, part, j, t):
+        remote(part, part, self.rows_send.at[0], self.rows_arrive.at[j, t], self.chain(0)).wait_recv()
+
+    def load(self, n):
+        source = (self.tokens_in, self.angles_in, self.taps_in)[n]
+        target = (self.tokens, self.angles, self.taps)[n]
+        return pltpu.make_async_copy(source, target, self.load_sems.at[n])
 
     def near_rows(self):
         zh, zl, y, x, c = self.at
         j = x * 2 + c
-        self.rows_copy(0, 1).start()
+        share = self.rows.shape[0]
+        self.load(0).wait()
+        tokens = self.tokens[...].astype(jnp.float32)
+        scaled = tokens * lax.rsqrt(jnp.mean(tokens * tokens, axis=-1, keepdims=True) + rms_eps)
+        self.rows[...] = (scaled * self.norm_gain[...]).astype(self.rows.dtype)
 
         @pl.when(c == zh)
         def _():
-            pltpu.make_async_copy(self.rows, self.block(j), self.rows_arrive.at[j]).start()
+            self.normed[pl.ds(pl.multiple_of(j * share, share), share)] = self.rows[...]
+
+        self.near_copy_of_rows(1).start()
+        pl.when(c != zh)(lambda: self.near_copy_of_rows(0).start())
+
+    def tables(self):
+        self.load(1).wait()
+        self.load(2).wait()
+        turn_cosine = self.turns[0, pl.ds(self.link, 1)]
+        turn_sine = self.turns[1, pl.ds(self.link, 1)]
+        cosine, sine = self.angles[0], self.angles[1]
+        self.cosine[...] = cosine * turn_cosine - sine * turn_sine
+        self.sine[...] = sine * turn_cosine + cosine * turn_sine
+
+    def relay_rows(self, t):
+        zh, zl, y, x, c = self.at
 
         @pl.when(c != zh)
         def _():
-            self.rows_copy(0, 0).start()
-
-    def relay_rows(self):
-        zh, zl, y, x, c = self.at
+            for core in range(2):
+                j = x * 2 + core
+                self.rows_landed(self.strip(j, t), j, t)
+                self.onward_strip(core, t).start()
+
+    def all_rows(self):
+        zh, zl, y, x, c = self.at
+
+        @pl.when(c == zh)
+        def _():
+            for j in range(4):
+                pl.when(x * 2 + c != j)(lambda: self.rows_landed(self.block(j), j, 0))
 
         @pl.when(c != zh)
         def _():
             for core in range(2):
-                self.block_arrived(x * 2 + core)
-                self.rows_onward(core).start()
-
-    def all_rows(self):
-        zh, zl, y, x, c = self.at
-        for j in range(4):
-            pl.when(jnp.logical_or(c == zh, x != j // 2))(lambda: self.block_arrived(j))
+                for t in range(STRIPS):
+                    j = (1 - x) * 2 + core
+                    self.rows_landed(self.strip(j, t), j, t)
 
     def drain_rows(self):
         zh, zl, y, x, c = self.at
-        self.rows_copy(0, 1).wait_send()
-        self.rows_copy(1, 0).wait_send()
+        self.near_copy_of_rows(1).wait_send()
+        for t in range(STRIPS):
+            self.far_strip(t).wait_send()
 
         @pl.when(c != zh)
         def _():
-            self.rows_copy(0, 0).wait_send()
-            self.rows_onward(0).wait_send()
-            self.rows_onward(1).wait_send()
-
-
-    def project(self, k, weights):
-        wide = weights.shape[2] // 2
-        for part in range(2):
-            columns = pl.ds(part * wide, wide)
-            self.products[k, :, columns] = jnp.dot(
-                self.normed[...], weights[k, :, columns], preferred_element_type=jnp.float32
-            ).astype(self.products.dtype)
-
-    def rotate(self, unit, target, scale):
+            self.near_copy_of_rows(0).wait_send()
+            for core in range(2):
+                for t in range(STRIPS):
+                    self.onward_strip(core, t).wait_send()
+
+
+    def project(self, k, weights, part, parts):
+        wide = weights.shape[2] // parts
+        columns = pl.ds(part * wide, wide)
+        self.products[k, :, columns] = jnp.dot(
+            self.normed[...], weights[k, :, columns], preferred_element_type=jnp.float32
+        ).astype(self.products.dtype)
+
+    def rotate(self, unit, target, scale, slot, slots):
         wide = KEY // 2
 
         def rows(first):
@@ -601,7 +656,7 @@
                 target[lines, low] = ((front * cosine - back * sine) * scale).astype(target.dtype)
                 target[lines, high] = ((front * sine + back * cosine) * scale).astype(target.dtype)
 
-        self.by_rows(128, rows)
+        self.by_rows(rows, slot, slots)
 
     def contribute(self, head):
         columns = pl.ds(head * KEY, KEY)
@@ -680,7 +735,7 @@
 
         self.others(arrived)
 
-    def inside(self, head):
+    def inside(self, head, slot, slots):
         columns = pl.ds(head * KEY, KEY)
         decay = self.log_decay(head)
 
@@ -695,9 +750,9 @@
                 scores, self.products[1 + head], preferred_element_type=jnp.float32
             )
 
-        self.by_rows(128, rows)
-
-    def finish_head(self, head):
+        self.by_rows(rows, slot, slots)
+
+    def finish_head(self, head, slot, slots):
         columns = pl.ds(head * KEY, KEY)
         decay = self.log_decay(head)
 
@@ -717,10 +772,10 @@
             result = centred * lax.rsqrt(wide + group_eps) * jax.nn.silu(switch)
             self.hidden[lines, pl.ds(head * VAL, VAL)] = result.astype(self.hidden.dtype)
 
-        self.by_rows(128, rows)
-
-
-    def glu(self):
+        self.by_rows(rows, slot, slots)
+
+
+    def glu(self, slot=0, slots=1):
         lead = self.halo_in.shape[0]
 
         def rows(first):
@@ -730,7 +785,7 @@
             gated = (value * jax.nn.sigmoid(switch)).astype(jnp.bfloat16)
             self.padded[pl.ds(pl.multiple_of(first + lead, 8), 128)] = gated.astype(jnp.float32)
 
-        self.by_rows(128, rows)
+        self.by_rows(rows, slot, slots)
         self.halo_out[...] = self.padded[pl.ds(self.count, lead)].astype(jnp.bfloat16)
         self.padded[pl.ds(self.count + lead, 8)] = jnp.zeros(
             (8, self.padded.shape[1]), jnp.float32
@@ -747,7 +802,7 @@
             self.chain(following),
         )
 
-    def convolve(self):
+    def halo(self):
         lead = self.halo_in.shape[0]
         channels = self.padded.shape[1]
 
@@ -760,11 +815,13 @@
         def _():
             self.padded[pl.ds(0, lead)] = jnp.zeros((lead, channels), jnp.float32)
 
+    def convolve(self, slot, slots):
+        lead = self.halo_in.shape[0]
+        channels = self.padded.shape[1]
         size = 64
         lanes = 128
 
-        def body(n, carry):
-            first = pl.multiple_of(n * size, size)
+        def rows(first):
             for part in range(channels // lanes):
                 columns = pl.ds(part * lanes, lanes)
                 spot = pl.multiple_of(self.rank * channels + part * lanes, lanes)
@@ -783,11 +840,10 @@
                         group = pltpu.roll(group, size + 8 - low, 0)
                     total = group[:size] if total is None else total + group[:size]
                 self.summed[pl.ds(first, size), columns] = total
-            return carry
-
-        lax.fori_loop(0, self.count // size, body, 0)
-
-    def finish_convolution(self):
+
+        self.by_rows(rows, slot, slots, size)
+
+    def finish_convolution(self, slot, slots):
         channels = self.padded.shape[1]
         spot = pl.ds(pl.multiple_of(self.rank * channels, channels), channels)
         gain, shift = self.gain[:, spot], self.shift[:, spot]
@@ -804,7 +860,7 @@
             target = pl.ds(self.heads * VAL, channels)
             self.hidden[lines, target] = result.astype(self.hidden.dtype)
 
-        self.by_rows(128, rows)
+        self.by_rows(rows, slot, slots)
 
 
     def x_copy(self, n):
@@ -845,7 +901,8 @@
         tile = self.sent.shape[2]
         n = j * 4 + q
         pair = self.sent.shape[1]
-        total = contract(self.hidden[...], weights[j, pl.ds(q * tile, tile)])
+        lines = pl.ds(pl.multiple_of(q * tile, tile), tile)
+        total = contract(self.hidden[...], weights[j, lines])
         low, high = total[:pair], total[pair:]
         self.kept[n] = jnp.where(x == 0, low, high)
         self.sent[n] = jnp.where(x == 0, high, low).astype(self.sent.dtype)
@@ -920,7 +977,8 @@
     units = len(layout)
     total = units + 2
 
-    layer.near_rows()
+    for n in range(3):
+        layer.load(n).start()
     for k, (which, first) in enumerate(layout):
         inward.load(k, blocks[which].at[:, pl.ds(first, inward.source.shape[2])], None)
     for k, parts in enumerate(out_layout):
@@ -929,11 +987,6 @@
             lines = pl.ds(row, outward.depth)
             outward.load(k, ref.at[lines], pl.ds(column, ref.shape[1]))
 
-    for k in range(AHEAD):
-        inward.begin(k)
-        if k == ROWS_AFTER:
-            layer.rows_copy(1, 0).start()
-
     def at_unit(k, what):
         @pl.when(jnp.logical_and(k >= 0, k < units))
         def _():
@@ -943,64 +996,123 @@
         def _():
             what(outward, k - units)
 
+    def first_sends(own, ahead):
+        for k in range(ahead):
+            if k < units:
+                inward.begin(k, own)
+            else:
+                outward.begin(k - units, own)
+
+    pl.when(inward.is_own)(lambda: first_sends(True, OWN_AHEAD))
+    pl.when(jnp.logical_not(inward.is_own))(lambda: first_sends(False, FAR_AHEAD))
+    layer.near_rows()
+    layer.far_strip(0).start()
+
+    def next_sends(i):
+        @pl.when(inward.is_own)
+        def _():
+            at_unit(i + OWN_AHEAD, lambda gather, k: gather.begin(k, True))
+
+        @pl.when(jnp.logical_not(inward.is_own))
+        def _():
+            at_unit(i + FAR_AHEAD, lambda gather, k: gather.begin(k, False))
+
+    inside, finish_head = layer.inside, layer.finish_head
+    key_scale = KEY ** (-0.5)
     after = (
-        (lambda: layer.rotate(0, layer.keys, KEY ** (-0.5)),),
-        (lambda: layer.contribute(0),),
-        (lambda: layer.contribute(1), layer.send_slices),
-        (lambda: layer.rotate(3, layer.queries, 1.0), layer.scan),
-        (lambda: layer.inside(0),),
-        (layer.glu, lambda: layer.inside(1)),
-        (layer.convolve,),
-        (layer.finish_convolution, layer.state_arrived, lambda: layer.finish_head(0)),
-        (lambda: layer.finish_head(1),),
+        (lambda n: layer.rotate(0, layer.keys, key_scale, n, 2),) * 2,
+        (lambda n: layer.contribute(0), None),
+        (lambda n: (layer.contribute(1), layer.send_slices()), None),
+        (lambda n: layer.rotate(3, layer.queries, 1.0, n, 2),) * 2,
+        (lambda n: (layer.scan(), inside(0, 0, 1)), None),
+        (lambda n: layer.glu(), lambda n: inside(1, 0, 1)),
+        (lambda n: (layer.halo(), layer.convolve(0, 1)), None),
+        (lambda n: layer.finish_convolution(0, 1), None),
+        (
+            lambda n: layer.state_arrived(),
+            lambda n: (finish_head(0, 0, 1), finish_head(1, 0, 1)),
+        ),
     )
 
+    def compute(k, carry):
+        inward.complete_own(k)
+        inward.complete_far(k)
+        layer.project(k, inward.full, 0, 2)
+        layer.project(k, inward.full, 1, 2)
+        for unit, events in enumerate(after):
+
+            @pl.when(k == unit)
+            def _():
+                for n, event in enumerate(events):
+                    if event is not None:
+                        event(n)
+
+        return carry
+
+    def relay(k, number):
+        at_unit(k, lambda gather, k: gather.stage(k, number))
+
+    for number in (0, 1, 4):
+        for k in range(LEADS[number]):
+            relay(k, number)
+
+    layer.tables()
+
+    def ready(i):
+        return jnp.clip(2 * (i - START), 0, jnp.clip(i + 1 - BEHIND, 0, units))
+
     def step(i, carry):
-        for number in range(3):
-            at_unit(i - LAGS[number], lambda gather, k: gather.stage(k, number))
-        at_unit(i + AHEAD, lambda gather, k: gather.begin(k))
-        pl.when(i == ROWS_RELAY)(layer.relay_rows)
-        done = i - LAGS[3]
-        pl.when(done == 0)(layer.all_rows)
-
-        @pl.when(jnp.logical_and(done >= 0, done < units))
-        def _():
-            inward.complete(done)
-            layer.project(done, inward.full)
-
-        for k, events in enumerate(after):
-
-            @pl.when(done == k)
-            def _():
-                for event in events:
-                    event()
-
+        relay(i + LEADS[0], 0)
+        relay(i + LEADS[1], 1)
+        pl.when(jnp.logical_and(i >= 0, i < STRIPS - 1))(lambda: layer.far_strip(i + 1).start())
+        next_sends(i)
+
+        @pl.when(jnp.logical_and(i >= ROWS_RELAY, i < ROWS_RELAY + STRIPS))
+        def _():
+            layer.relay_rows(i - ROWS_RELAY)
+
+        relay(i, 2)
+        relay(i + LEADS[4], 4)
+        relay(i - 1, 3)
+        pl.when(i == START + 1)(layer.all_rows)
+        lax.fori_loop(ready(i - 1), ready(i), compute, 0)
         return carry
 
-    lax.fori_loop(0, units + LAGS[3], step, 0)
-
-    def output(j):
-        outward.complete(j)
+    lax.fori_loop(0, units + 1, step, 0)
+    lax.fori_loop(ready(units), units, compute, 0)
+
+    zh = layer.at[0]
+
+    def tiles(j, half, what):
+        for m in range(2):
+            what(j, half * 2 + m)
+
+    def multiply(j, q):
+        layer.multiply(j, q, outward.full)
+
+    def join(j, q):
+        layer.join(j * 4 + q)
+
+    for k in range(units + 1 + LEADS[4], total):
+        relay(k, 4)
+    outward.complete_own(0)
+    tiles(0, zh, multiply)
+    relay(units, 3)
+    outward.complete_own(1)
+    tiles(1, zh, multiply)
+    relay(units + 1, 2)
+    outward.complete_far(0)
+    tiles(0, 1 - zh, multiply)
+    tiles(0, zh, join)
+    tiles(1, zh, join)
+    relay(units + 1, 3)
+    outward.complete_far(1)
+    tiles(1, 1 - zh, multiply)
+    tiles(0, 1 - zh, join)
+    tiles(1, 1 - zh, join)
+    for j in range(2):
         for q in range(4):
-            layer.multiply(j, q, outward.full)
-
-    def late_stages(j):
-        for number in range(3):
-            if units + j + LAGS[number] >= units + LAGS[3]:
-                outward.stage(j, number)
-
-    late_stages(0)
-    output(0)
-    late_stages(1)
-    for n in range(4):
-        layer.join(n)
-    output(1)
-    for q in range(4):
-        layer.close(0, q)
-    for n in range(4, 8):
-        layer.join(n)
-    for q in range(4):
-        layer.close(1, q)
+            layer.close(j, q)
 
     def finish(gather):
         def body(k, carry):
@@ -1014,15 +1126,20 @@
     layer.drain()
 
 
-def whole_layer(rows, cosine, sine, taps, gain, shift, blocks):
+def whole_layer(tokens, norm_gain, taps, gain, shift, blocks):
     depth, width = blocks[0].shape
-    share, model = rows.shape
+    share, model = tokens.shape
     layout = []
     for which, block in enumerate(blocks[:7]):
         layout += [(which, first) for first in range(0, block.shape[1], width)]
     units = len(layout)
-    shares, dtype = 8, rows.dtype
+    shares, dtype = 8, tokens.dtype
     span = 4 * share
+    wide = KEY // 2
+    frequency = rope_base ** (-np.arange(wide) / wide)
+    angles = [np.arange(span)[:, None] * frequency]
+    angles += [span * np.arange(shares)[:, None] * frequency]
+    angles, turns = (np.stack([np.cos(a), np.sin(a)]).astype(np.float32) for a in angles)
     inner_width = blocks[7].shape[1] + blocks[8].shape[1]
     half_depth = depth // 2
     out_layout = [
@@ -1038,10 +1155,17 @@
     return pl.pallas_call(
         lambda *refs: layer_kernel(layout, out_layout, *refs),
         out_shape=jax.ShapeDtypeStruct((share, model), dtype),
-        in_specs=[pl.BlockSpec(memory_space=pl.ANY)] * 10
-        + [pl.BlockSpec(memory_space=pltpu.VMEM)] * 5,
+        in_specs=[pl.BlockSpec(memory_space=pl.ANY)] * 11
+        + [pl.BlockSpec(memory_space=pltpu.VMEM), pl.BlockSpec(memory_space=pl.ANY)]
+        + [pl.BlockSpec(memory_space=pltpu.VMEM)] * 3,
         out_specs=pl.BlockSpec(memory_space=pltpu.VMEM),
         scratch_shapes=[
+            pltpu.VMEM((share, model), dtype),
+            pltpu.VMEM(angles.shape, jnp.float32),
+            pltpu.VMEM(taps.shape, jnp.float32),
+            pltpu.VMEM((share, model), dtype),
+            pltpu.VMEM((span, wide), jnp.float32),
+            pltpu.VMEM((span, wide), jnp.float32),
             pltpu.VMEM((span, model), dtype),
             pltpu.VMEM((units, span, width), dtype),
             pltpu.VMEM((span, width), dtype),
@@ -1062,18 +1186,19 @@
             pltpu.VMEM((tiles, 2 * share, tile), dtype),
             pltpu.VMEM((tiles, share, tile), dtype),
             pltpu.VMEM((tiles, share, tile), dtype),
-            sem((5,)),
-            sem((4,)),
+            sem((2 + 3 * STRIPS,)),
+            sem((4, STRIPS)),
             sem((2, shares)),
             sem((2, shares)),
             sem((2,)),
             sem((6, tiles)),
+            sem((3,)),
         ]
         + gather_scratch(units, depth, width, shares, dtype)
         + gather_scratch(2, half_depth, inner_width, shares, dtype),
         compiler_params=pltpu.CompilerParams(has_side_effects=True, vmem_limit_bytes=60 << 20),
         name="layer",
-    )(*blocks, rows, cosine, sine, taps, gain, shift)
+    )(*blocks, tokens, angles, turns, taps, norm_gain, gain, shift)
 
 
 def local_squares(
@@ -1092,19 +1217,11 @@
     retain_output,
     convolve_output,
 ):
-    chain_rank = lax.axis_index(CHAIN)
-    normed = rms_normalize(tokens, norm_gain)
-    row_count = normed.shape[0] * 4
-    half_width = KEY // 2
-    frequency = rope_base ** (-jnp.arange(half_width, dtype=jnp.float32) / half_width)
-    positions = chain_rank * row_count + jnp.arange(row_count, dtype=jnp.int32)
-    angles = positions.astype(jnp.float32)[:, None] * frequency
     blocks = (key_weight, value_weight, query_weight, unit_value, unit_gate, convolve_gate)
     blocks += (retain_gate, retain_output, convolve_output)
     return whole_layer(
-        normed,
-        jnp.cos(angles),
-        jnp.sin(angles),
+        tokens,
+        norm_gain[None],
         filter_taps,
         layer_gain[None],
         layer_shift[None],

time: 204 us -> 189 us (0.926)
  Pallas kernels: 198 us -> 185 us
  other arithmetic: 4.13 us -> 0 us
    pallas_call x1, Pallas kernels: 198 us -> 185 us  [whole_layer(): pl.pallas_call(lambda *refs: layer_kernel(layout, out_layout, *refs), out...]
where the time goes in v3:
time: 189 us; the launch traced here: 187 us
  Pallas kernels  185 us (98%)
    pallas_call x1, Pallas kernels, whole_layer(): pl.pallas_call(lambda *refs: layer_kernel(layout, out_layout, *refs), out...  185 us

profile of v3, /device:TPU:9, one launch (start us, length us, event | category | flops | bytes accessed | tf_op | source)
XLA Modules:
  0.0 187.1 jit_solution(8129645519915372658)
XLA Ops:
  0.0 185.3 %layer.1 = bf16[128,2048]{1,0:T(8,128)(2,1)} custom-call(bf16[256,512]{1,0:T(8,128)(2,1)} %refs_0_.1, bf16[256,1024]{1,0:T(8,128)(2,1)} %refs_1_.1, bf16[256,512]{1,0:T(8,128)(2,1)} %refs_2_.1, bf16[256,512]{1,0:T(8,128)(2,1)} %refs_3_.1, bf16[256,512]{1,0:T(8,128)(2,1)} %refs_4_.1, bf16[256,512]{1,0:T(8,128)(2,1)} %refs_5_.1, bf16[256,1024]{1,0:T(8,128)(2,1)} %refs_6_.1, ...), custom_call_target="tpu_custom_call" | custom-call | tf_op jit(solution)/shard_map/layer/pallas_call | solution.py:1155
  185.3 1.9 %copy.18 = bf16[128,2048]{1,0:T(8,128)(2,1)} copy(bf16[128,2048]{1,0:T(8,128)(2,1)} %layer.1) | data formatting | bytes 1048576

commit v4 on v3

--- a/solution.py
+++ b/solution.py
@@ -235,6 +235,20 @@
 
 def place():
     return tuple(lax.axis_index(name) for name in SQUARE)
+
+
+def meet():
+    zh, zl, y, x, c = place()
+    barrier = pltpu.get_barrier_semaphore()
+    peers = []
+    for n in range(1, 16):
+        flips = [(n >> bit) & 1 for bit in range(4)]
+        a, b, d, e = (1 - v if flip else v for v, flip in zip((zh, zl, y, c), flips))
+        peers.append((a, b, d, x, e))
+    peers += [(zh, zl, y, 1 - x, c), (zh, zl, y, 1 - x, 1 - c)]
+    for peer in peers:
+        pl.semaphore_signal(barrier, inc=1, device_id=peer, device_id_type=MESH)
+    pl.semaphore_wait(barrier, len(peers))
 
 
 class Gather:
@@ -996,6 +1010,8 @@
         def _():
             what(outward, k - units)
 
+    meet()
+
     def first_sends(own, ahead):
         for k in range(ahead):
             if k < units:
@@ -1024,9 +1040,9 @@
         (lambda n: layer.contribute(0), None),
         (lambda n: (layer.contribute(1), layer.send_slices()), None),
         (lambda n: layer.rotate(3, layer.queries, 1.0, n, 2),) * 2,
-        (lambda n: (layer.scan(), inside(0, 0, 1)), None),
+        (lambda n: inside(0, 0, 1), None),
         (lambda n: layer.glu(), lambda n: inside(1, 0, 1)),
-        (lambda n: (layer.halo(), layer.convolve(0, 1)), None),
+        (lambda n: layer.scan(), lambda n: (layer.halo(), layer.convolve(0, 1))),
         (lambda n: layer.finish_convolution(0, 1), None),
         (
             lambda n: layer.state_arrived(),
@@ -1196,7 +1212,9 @@
         ]
         + gather_scratch(units, depth, width, shares, dtype)
         + gather_scratch(2, half_depth, inner_width, shares, dtype),
-        compiler_params=pltpu.CompilerParams(has_side_effects=True, vmem_limit_bytes=60 << 20),
+        compiler_params=pltpu.CompilerParams(
+            has_side_effects=True, collective_id=0, vmem_limit_bytes=60 << 20
+        ),
         name="layer",
     )(*blocks, tokens, angles, turns, taps, norm_gain, gain, shift)
 

time: 189 us -> 183 us (0.968); the launches traced: 187 us -> 183 us
  Pallas kernels: 185 us -> 181 us
    pallas_call x1, Pallas kernels: 185 us -> 181 us  [whole_layer(): pl.pallas_call(lambda *refs: layer_kernel(layout, out_layout, *refs), out...]
where the time goes in v4:
time: 183 us
  Pallas kernels  181 us (99%)
  local copies, waits for them, and re-layouts  1.88 us (1%)
    pallas_call x1, Pallas kernels, whole_layer(): pl.pallas_call(lambda *refs: layer_kernel(layout, out_layout, *refs), out...  181 us

profile of v4, /device:TPU:9, one launch (start us, length us, event | category | flops | bytes accessed | tf_op | source)
XLA Modules:
  0.0 183.1 jit_solution(17269326796360797558)
XLA Ops:
  0.0 181.2 %layer.1 = bf16[128,2048]{1,0:T(8,128)(2,1)} custom-call(bf16[256,512]{1,0:T(8,128)(2,1)} %refs_0_.1, bf16[256,1024]{1,0:T(8,128)(2,1)} %refs_1_.1, bf16[256,512]{1,0:T(8,128)(2,1)} %refs_2_.1, bf16[256,512]{1,0:T(8,128)(2,1)} %refs_3_.1, bf16[256,512]{1,0:T(8,128)(2,1)} %refs_4_.1, bf16[256,512]{1,0:T(8,128)(2,1)} %refs_5_.1, bf16[256,1024]{1,0:T(8,128)(2,1)} %refs_6_.1, ...), custom_call_target="tpu_custom_call" | custom-call | tf_op jit(solution)/shard_map/layer/pallas_call | solution.py:1171
  181.2 1.9 %copy.18 = bf16[128,2048]{1,0:T(8,128)(2,1)} copy(bf16[128,2048]{1,0:T(8,128)(2,1)} %layer.1) | data formatting | bytes 1048576

commit v5 on v4

--- a/solution.py
+++ b/solution.py
@@ -248,7 +248,7 @@
     peers += [(zh, zl, y, 1 - x, c), (zh, zl, y, 1 - x, 1 - c)]
     for peer in peers:
         pl.semaphore_signal(barrier, inc=1, device_id=peer, device_id_type=MESH)
-    pl.semaphore_wait(barrier, len(peers))
+    return lambda: pl.semaphore_wait(barrier, len(peers))
 
 
 class Gather:
@@ -991,8 +991,7 @@
     units = len(layout)
     total = units + 2
 
-    for n in range(3):
-        layer.load(n).start()
+    met = meet()
     for k, (which, first) in enumerate(layout):
         inward.load(k, blocks[which].at[:, pl.ds(first, inward.source.shape[2])], None)
     for k, parts in enumerate(out_layout):
@@ -1010,7 +1009,9 @@
         def _():
             what(outward, k - units)
 
-    meet()
+    for n in range(3):
+        layer.load(n).start()
+    met()
 
     def first_sends(own, ahead):
         for k in range(ahead):

time: 183 us -> 183 us (level)
  no operation moved by 1% of the time
where the time goes in v5:
time: 183 us
  Pallas kernels  181 us (99%)
  local copies, waits for them, and re-layouts  1.88 us (1%)
    pallas_call x1, Pallas kernels, whole_layer(): pl.pallas_call(lambda *refs: layer_kernel(layout, out_layout, *refs), out...  181 us

profile of v5, /device:TPU:9, one launch (start us, length us, event | category | flops | bytes accessed | tf_op | source)
XLA Modules:
  0.0 183.0 jit_solution(12726757796477035253)
XLA Ops:
  0.0 181.1 %layer.1 = bf16[128,2048]{1,0:T(8,128)(2,1)} custom-call(bf16[256,512]{1,0:T(8,128)(2,1)} %refs_0_.1, bf16[256,1024]{1,0:T(8,128)(2,1)} %refs_1_.1, bf16[256,512]{1,0:T(8,128)(2,1)} %refs_2_.1, bf16[256,512]{1,0:T(8,128)(2,1)} %refs_3_.1, bf16[256,512]{1,0:T(8,128)(2,1)} %refs_4_.1, bf16[256,512]{1,0:T(8,128)(2,1)} %refs_5_.1, bf16[256,1024]{1,0:T(8,128)(2,1)} %refs_6_.1, ...), custom_call_target="tpu_custom_call" | custom-call | tf_op jit(solution)/shard_map/layer/pallas_call | solution.py:1172
  181.1 1.9 %copy.18 = bf16[128,2048]{1,0:T(8,128)(2,1)} copy(bf16[128,2048]{1,0:T(8,128)(2,1)} %layer.1) | data formatting | bytes 1048576
